TPU v7x, 256 devices: a whole 4x4x8 slice. The times are simulated.
256 devices in a mesh: kv: 32 (over z, x), tp: 8 (over y, core).
Axes of the slice: x: 4, y: 4, z: 8, core: 2. Of those that a mesh axis runs over, the one named last changes fastest.
Arguments:
- tokens: bfloat16 [256, 4, 4096], P(None, None, 'kv')
- norm_gain: float32 [4096], replicated, may hold values from 0.1 to 1.9
- w_query: bfloat16 [4096, 4096], P('kv', 'tp'), may hold values from -0.09375 to 0.09375
- w_key: bfloat16 [4096, 4096], P('kv', 'tp'), may hold values from -0.09375 to 0.09375
- w_value: bfloat16 [4096, 4096], P('kv', 'tp'), may hold values from -0.09375 to 0.09375
- w_gate: bfloat16 [4096, 4096], P('kv', 'tp'), may hold values from -0.09375 to 0.09375
- w_decay: bfloat16 [4096, 32], replicated, may hold values from -0.09375 to 0.09375
- w_beta: bfloat16 [4096, 32], replicated, may hold values from -0.09375 to 0.09375
- decay_rate: float32 [32], replicated, may hold values from 0.02 to 3
- head_gain: float32 [128], replicated, may hold values from 0.1 to 1.9
- w_out: bfloat16 [4096, 4096], P('tp', 'kv'), may hold values from -0.09375 to 0.09375
- state: float32 [256, 32, 128, 128], P('kv', 'tp'), may hold values from -0.4 to 0.4
- prev_keys: bfloat16 [256, 32, 4, 128], P('kv', 'tp'), may hold values from -6 to 6
- prev_values: bfloat16 [256, 32, 4, 128], P('kv', 'tp'), may hold values from -6 to 6
- prev_log_decay: float32 [256, 32, 4], P('kv', 'tp'), may hold values from -0.7 to -0.02
- prev_beta: float32 [256, 32, 4], P('kv', 'tp'), may hold values from 0.1 to 0.9
- accepted: int32 [256], P('kv'), may hold values from 0 to 4
Outputs:
- mixed: bfloat16 [256, 4, 4096], P('tp', None, 'kv')
- carried: float32 [256, 32, 128, 128], P('kv', 'tp')
All inputs are finite; a program needn't handle non-finite values.
Results may differ from a plain program's by a relative error of at most 0.0069.
Values may be sent and summed in bfloat16 or wider, within the bound.
A program may use at most 128 MiB of HBM per device.

v0:
```python
import jax
import jax.numpy as jnp
from jax import lax
from jax.sharding import PartitionSpec as P

epsilon = 1e-06


def side_by_side(arrays, axis, dim, along):
    ends, at = ([], 0)
    for a in arrays[:-1]:
        at += a.shape[along]
        ends.append(at)
    both = jnp.concatenate(arrays, axis=along)
    return tuple(jnp.split(lax.all_gather(both, axis, axis=dim, tiled=True), ends, axis=along))


def copy_for_each(shard, axis):
    copies = jnp.broadcast_to(shard, (lax.axis_size(axis), *shard.shape))
    return lax.all_to_all(copies, axis, split_axis=0, concat_axis=0, tiled=True)


def in_order(tiles, dim):
    dims = list(tiles.shape[1:])
    dims[dim] *= tiles.shape[0]
    return jnp.moveaxis(tiles, 0, dim).reshape(dims)


def gathered_copies(shard, axis, dim):
    tiles = copy_for_each(shard, axis)
    return in_order(tiles, dim)


def in_blocks(shard, dim, size):
    before, after = (shard.shape[:dim], shard.shape[dim + 1 :])
    return jnp.moveaxis(shard.reshape(*before, size, -1, *after), dim, 0)


def summed_on_arrival(shard, axis, dim):
    size = lax.axis_size(axis)
    tiles = lax.all_to_all(in_blocks(shard, dim, size), axis, 0, 0, tiled=True)
    return jnp.sum(tiles, axis=0)


def unit_rows(values):
    return values * lax.rsqrt(jnp.sum(values * values, axis=-1, keepdims=True) + epsilon)


def apply_update(matrix, keyvec, valvec, logd, strength):
    decayed = jnp.exp(logd)[..., None, None] * matrix
    predicted = jnp.einsum("bhde,bhd->bhe", decayed, keyvec, precision=lax.Precision.HIGHEST)
    change = strength[..., None] * (valvec - predicted)
    return decayed + jnp.einsum("bhd,bhe->bhde", keyvec, change, precision=lax.Precision.HIGHEST)


def per_device(
    tokens,
    norm_gain,
    w_query,
    w_key,
    w_value,
    w_gate,
    w_decay,
    w_beta,
    decay_rate,
    head_gain,
    w_out,
    state,
    prev_keys,
    prev_values,
    prev_log_decay,
    prev_beta,
    accepted,
):
    f32 = jnp.float32
    seq_here, heads_here, key_size, value_size = state.shape
    props = tokens.shape[1]
    width_here = tokens.shape[2]
    dmodel = w_decay.shape[0]
    head_start = lax.axis_index("tp") * heads_here
    decay_cols = lax.dynamic_slice_in_dim(w_decay, head_start, heads_here, 1)
    beta_cols = lax.dynamic_slice_in_dim(w_beta, head_start, heads_here, 1)
    rate_here = lax.dynamic_slice_in_dim(decay_rate, head_start, heads_here, 0)
    vwidth = heads_here * value_size
    own_rows = lax.all_to_all(tokens, "kv", split_axis=0, concat_axis=2, tiled=True)
    features = own_rows.reshape(seq_here * props, dmodel).astype(f32)
    scale = lax.rsqrt(jnp.mean(features * features, axis=1, keepdims=True) + epsilon)
    normed = (features * scale * norm_gain).astype(jnp.bfloat16)
    pieces = side_by_side((w_query, w_key, w_value, w_gate), "kv", 0, 1)
    qraw, kraw, vraw, zraw = tuple(
        (jnp.dot(normed, piece, preferred_element_type=f32) for piece in pieces)
    )
    araw = jnp.dot(normed, decay_cols, preferred_element_type=f32)
    braw = jnp.dot(normed, beta_cols, preferred_element_type=f32)
    query = unit_rows(
        jax.nn.silu(qraw).reshape(seq_here, props, heads_here, key_size)
    ) * key_size ** (-0.5)
    keyrow = unit_rows(jax.nn.silu(kraw).reshape(seq_here, props, heads_here, key_size))
    value = jax.nn.silu(vraw).reshape(seq_here, props, heads_here, value_size)
    beta = jax.nn.sigmoid(braw).reshape(seq_here, props, heads_here)
    logdecay = (-rate_here * jax.nn.softplus(araw)).reshape(seq_here, props, heads_here)
    old_keys = unit_rows(prev_keys.astype(f32))
    old_values = prev_values.astype(f32)
    matrix = state
    for proposal in range(props):
        keep = (proposal < accepted).astype(f32)[:, None]
        matrix = apply_update(
            matrix,
            old_keys[:, :, proposal],
            old_values[:, :, proposal],
            prev_log_decay[:, :, proposal] * keep,
            prev_beta[:, :, proposal] * keep,
        )
    carried = matrix
    results = []
    for proposal in range(props):
        matrix = apply_update(
            matrix,
            keyrow[:, proposal],
            value[:, proposal],
            logdecay[:, proposal],
            beta[:, proposal],
        )
        results.append(
            jnp.einsum("bhde,bhd->bhe", matrix, query[:, proposal], precision=lax.Precision.HIGHEST)
        )
    attended = jnp.stack(results, axis=1)
    zgate = zraw.reshape(seq_here, props, heads_here, value_size)
    headout = attended * lax.rsqrt(jnp.mean(attended * attended, axis=-1, keepdims=True) + epsilon)
    headout = (
        (headout * head_gain * jax.nn.silu(zgate))
        .astype(jnp.bfloat16)
        .reshape(seq_here * props, vwidth)
    )
    terms = jnp.dot(gathered_copies(headout, "kv", 0), w_out, preferred_element_type=f32)
    mixed = summed_on_arrival(terms, "tp", 0)
    return (mixed.reshape(-1, props, width_here).astype(jnp.bfloat16), carried)


def solution(mesh):
    placed = (
        P(None, None, "kv"),
        P(),
        P("kv", "tp"),
        P("kv", "tp"),
        P("kv", "tp"),
        P("kv", "tp"),
        P(),
        P(),
        P(),
        P(),
        P("tp", "kv"),
        P("kv", "tp", None, None),
        P("kv", "tp", None, None),
        P("kv", "tp", None, None),
        P("kv", "tp", None),
        P("kv", "tp", None),
        P("kv"),
    )
    return jax.shard_map(
        per_device,
        mesh=mesh,
        in_specs=placed,
        out_specs=(P("tp", None, "kv"), P("kv", "tp", None, None)),
        check_vma=False,
    )
```

profile of v0, /device:TPU:1, one launch (start us, length us, event | category | flops | bytes accessed | tf_op | source)
XLA Modules:
  0.0 259.0 jit_solution(12432108467054536670)
XLA Ops:
  7.3 2.1 pad_maximum_fusion
  9.4 11.9 %all-to-all-start = ((bf16[256,4,128]{2,1,0:T(4,128)(2,1)}), bf16[256,4,128]{2,1,0:T(4,128)(2,1)S(1)}, u32[]{:S(2)}, u32[]{:S(2)}) async-start(bf16[256,4,128]{2,1,0:T(4,128)(2,1)} %param.17), calls=%async_computation | async-start | bytes 524288 | tf_op jit(solution)/shard_map/all_to_all | solution.py:85
  22.4 2.0 fusion.18
  24.5 2.2 fusion.59
  26.8 2.9 %fusion.20 = f32[8,4,1,128]{3,2,1,0:T(1,128)S(1)} fusion(f32[8,4,128]{2,1,0:T(4,128)S(1)} %subtract_multiply_fusion.2, f32[8,4,128]{2,1,0:T(4,128)S(1)} %bitcast.207, f32[8,4]{1,0:T(8,128)S(1)} %copy.87, f32[8,4,128,128]{3,2,1,0:T(8,128)S(1)} %copy-done.2, f32[8,4,128]{2,1,0:T(4,128)S(1)} %subtract_multiply_fusion.3, f32[8,4,128]{2,1,0:T(4,128)S(1)} %bitcast.211, ...), kind=kOutput, calls=%fused_computation.28 | convolution fusion | flops 9961472 | bytes 2207744 | tf_op jit(solution)/shard_map/bhde,bhd->bhe/dot_general | solution.py:51
  29.8 3.9 %fusion.21 = f32[8,4,1,128]{3,2,1,0:T(1,128)S(1)} fusion(f32[8,4,128]{2,1,0:T(4,128)S(1)} %subtract_multiply_fusion.1, f32[8,4,128]{2,1,0:T(4,128)S(1)} %bitcast.205, f32[8,4,128]{2,1,0:T(4,128)S(1)} %subtract_multiply_fusion.2, f32[8,4,128]{2,1,0:T(4,128)S(1)} %bitcast.208, f32[8,4]{1,0:T(8,128)S(1)} %copy.87, f32[8,4]{1,0:T(8,128)S(1)} %copy.86, ...), kind=kOutput, calls=%fused_computation.29 | convolution fusion | flops 11534336 | bytes 2244608 | tf_op jit(solution)/shard_map/bhde,bhd->bhe/dot_general | solution.py:51
  33.8 5.7 %multiply_add_fusion.3 = f32[8,4,128,128]{3,2,1,0:T(8,128)S(1)} fusion(f32[8,4,128]{2,1,0:T(4,128)S(1)} %subtract_multiply_fusion, f32[8,4,128]{2,1,0:T(4,128)S(1)} %bitcast.204, f32[8,4,128]{2,1,0:T(4,128)S(1)} %subtract_multiply_fusion.1, f32[8,4,128]{2,1,0:T(4,128)S(1)} %bitcast.206, f32[8,4,128]{2,1,0:T(4,128)S(1)} %subtract_multiply_fusion.2, ...), kind=kLoop, calls=%fused_computation.13 | loop fusion | flops 6291456 | bytes 4325888 | tf_op jit(solution)/shard_map/add | solution.py:53
  43.5 110.0 %all-gather.2.cloned.1.call-done = bf16[4096,2048]{1,0:T(8,128)(2,1)} async-done(((bf16[128,2048]{1,0:T(8,128)(2,1)}), bf16[4096,2048]{1,0:T(8,128)(2,1)}) %all-gather.2.cloned.1.call-update) | async-done | bytes 16777232 | tf_op jit(solution)/shard_map/all_gather | solution.py:15
  153.5 3.0 %divide_multiply_fusion = f32[32,512]{1,0:T(8,128)S(1)} fusion(bf16[32,4096]{1,0:T(8,128)(2,1)S(1)} %fusion.61, bf16[4096,2048]{1,0:T(8,128)(2,1)} %all-gather.2.cloned.1.call-done), kind=kOutput, calls=%fused_computation.89 | convolution fusion | flops 134283264 | bytes 4521984 | tf_op jit(solution)/shard_map/dot_general | solution.py:91
  156.8 3.0 %divide_multiply_fusion.1 = f32[32,512]{1,0:T(8,128)S(1)} fusion(bf16[32,4096]{1,0:T(8,128)(2,1)S(1)} %fusion.61, bf16[4096,2048]{1,0:T(8,128)(2,1)} %all-gather.2.cloned.1.call-done), kind=kOutput, calls=%fused_computation.90 | convolution fusion | flops 134283264 | bytes 4521984 | tf_op jit(solution)/shard_map/dot_general | solution.py:91
  159.9 3.0 %divide_multiply_fusion.2 = f32[32,512]{1,0:T(8,128)S(1)} fusion(bf16[32,4096]{1,0:T(8,128)(2,1)S(1)} %fusion.61, bf16[4096,2048]{1,0:T(8,128)(2,1)} %all-gather.2.cloned.1.call-done), kind=kOutput, calls=%fused_computation.92 | convolution fusion | flops 134283264 | bytes 4521984 | tf_op jit(solution)/shard_map/dot_general | solution.py:91
  162.9 4.4 %slice_bitcast_fusion = bf16[512,4096]{0,1:T(8,128)(2,1)} fusion(bf16[4096,2048]{1,0:T(8,128)(2,1)} %all-gather.2.cloned.1.call-done), kind=kLoop, calls=%fused_computation | loop fusion | bytes 8388608 | tf_op jit(solution)/shard_map/dot_general | solution.py:91
  167.3 6.4 %copy.104 = bf16[512,4096]{1,0:T(8,128)(2,1)} copy(bf16[512,4096]{0,1:T(8,128)(2,1)} %slice_bitcast_fusion) | data formatting | bytes 8388608 | tf_op jit(solution)/shard_map/dot_general | solution.py:91
  174.0 2.0 fusion.16
  176.1 2.2 fusion.22
  178.3 2.2 fusion.14
  180.6 2.9 %fusion.101 = f32[8,4,1,128]{3,2,1,0:T(1,128)S(1)} fusion(f32[8,4,128,1]{2,3,1,0:T(1,128)S(1)} %bitcast.252, f32[8,4,128,128]{3,2,1,0:T(8,128)S(1)} %multiply_add_fusion.3, f32[8,4,128]{2,1,0:T(4,128)S(1)} %fusion.85, f32[8,4,128]{2,1,0:T(4,128)S(1)} %get-tuple-element.8, f32[8,4]{1,0:T(8,128)S(1)} %bitcast.268, f32[8,4,128]{2,1,0:T(4,128)S(1)} %fusion.87, ...), kind=kOutput, calls=%fused_computation.157 | convolution fusion | flops 9437184 | bytes 2195712 | tf_op jit(solution)/shard_map/bhde,bhd->bhe/dot_general | solution.py:125
  183.5 2.9 %fusion.12 = f32[8,4,1,128]{3,2,1,0:T(1,128)S(1)} fusion(f32[8,4,128,1]{2,3,1,0:T(1,128)S(1)} %bitcast.238, f32[8,4]{1,0:T(8,128)S(1)} %bitcast.263, f32[8,4,128,128]{3,2,1,0:T(8,128)S(1)} %multiply_add_fusion.3, f32[8,4,128]{2,1,0:T(4,128)S(1)} %fusion.85, f32[8,4,128]{2,1,0:T(4,128)S(1)} %get-tuple-element.8, f32[8,4]{1,0:T(8,128)S(1)} %bitcast.269, ...), kind=kOutput, calls=%fused_computation.20 | convolution fusion | flops 9961472 | bytes 2195840 | tf_op jit(solution)/shard_map/bhde,bhd->bhe/dot_general | solution.py:51
  186.5 3.8 %fusion.23 = f32[8,4,1,128]{3,2,1,0:T(1,128)S(1)} fusion(f32[8,4,128,1]{2,3,1,0:T(1,128)S(1)} %bitcast.251, f32[8,4,128]{2,1,0:T(4,128)S(1)} %fusion.83, f32[8,4,128]{2,1,0:T(4,128)S(1)} %get-tuple-element.9, f32[8,4]{1,0:T(8,128)S(1)} %bitcast.264, f32[8,4,128,128]{3,2,1,0:T(8,128)S(1)} %multiply_add_fusion.3, f32[8,4,128]{2,1,0:T(4,128)S(1)} %fusion.85, ...), kind=kOutput, calls=%fused_computation.31 | convolution fusion | flops 11010048 | bytes 2228608 | tf_op jit(solution)/shard_map/bhde,bhd->bhe/dot_general | solution.py:125
  190.3 3.9 %fusion.10 = f32[8,4,1,128]{3,2,1,0:T(1,128)S(1)} fusion(f32[8,4,128,1]{2,3,1,0:T(1,128)S(1)} %bitcast.237, f32[8,4]{1,0:T(8,128)S(1)} %bitcast.261, f32[8,4,128]{2,1,0:T(4,128)S(1)} %fusion.83, f32[8,4,128]{2,1,0:T(4,128)S(1)} %get-tuple-element.9, f32[8,4]{1,0:T(8,128)S(1)} %bitcast.265, f32[8,4,128,128]{3,2,1,0:T(8,128)S(1)} %multiply_add_fusion.3, ...), kind=kOutput, calls=%fused_computation.18 | convolution fusion | flops 11534336 | bytes 2228736 | tf_op jit(solution)/shard_map/bhde,bhd->bhe/dot_general | solution.py:51
  194.3 5.2 %fusion.6 = f32[8,4,1,128]{3,2,1,0:T(1,128)S(1)} fusion(f32[8,4,128,1]{2,3,1,0:T(1,128)S(1)} %bitcast.250, f32[8,4,128]{2,1,0:T(4,128)S(1)} %fusion.81, f32[8,4,128]{2,1,0:T(4,128)S(1)} %get-tuple-element.6, f32[8,4]{1,0:T(8,128)S(1)} %bitcast.262, f32[8,4,128]{2,1,0:T(4,128)S(1)} %fusion.83, f32[8,4,128]{2,1,0:T(4,128)S(1)} %get-tuple-element.9, ...), kind=kOutput, calls=%fused_computation.7 | convolution fusion | flops 12582912 | bytes 2261504 | tf_op jit(solution)/shard_map/bhde,bhd->bhe/dot_general | solution.py:125
  199.9 3.5 %multiply_convert_fusion.1 = bf16[8,4,4,128]{3,0,2,1:T(8,128)(2,1)S(1)} fusion(bf16[4,128,4096,1]{2,1,0,3:T(8,128)(2,1)} %bitcast.196, bf16[8,4,32,128]{3,1,0,2:T(4,128)(2,1)S(1)} %fusion.62, f32[8,1,4,128]{3,0,2,1:T(8,128)S(1)} %bitcast.223, f32[8,1,4,128]{3,0,2,1:T(8,128)S(1)} %bitcast.221, f32[8,1,4,128]{3,0,2,1:T(8,128)S(1)} %bitcast.219, ...), kind=kOutput, calls=%fused_computation.85 | convolution fusion | flops 134397952 | bytes 4555776 | tf_op jit(solution)/shard_map/dot_general | solution.py:91
  203.6 30.9 %all_to_all.19 = bf16[32,32,512]{2,1,0:T(8,128)(2,1)S(1)} all-to-all(bf16[32,32,512]{2,1,0:T(8,128)(2,1)S(1)} %broadcast_in_dim.2), channel_id=1, replica_groups=mesh['kv'=32,'tp'=8] {'kv'}, dimensions={0} | all-to-all | bytes 2097152 | tf_op jit(solution)/shard_map/all_to_all | solution.py:20
  234.9 16.6 %all_to_all.20 = f32[8,128,128]{2,1,0:T(8,128)S(1)} all-to-all(f32[8,128,128]{2,1,0:T(8,128)S(1)} %fusion.66), channel_id=1, replica_groups=mesh['kv'=32,'tp'=8] {'tp'}, dimensions={0} | all-to-all | bytes 1048576 | tf_op jit(solution)/shard_map/all_to_all | solution.py:41
  (99 shorter events, 7.8 us)
Async XLA Ops:
  7.2 33.4 %copy-start = (bf16[4096,32]{0,1:T(8,128)(2,1)S(1)}, bf16[4096,32]{0,1:T(8,128)(2,1)}, u32[]{:S(2)}) copy-start(bf16[4096,32]{0,1:T(8,128)(2,1)} %param.24) | copy-start | bytes 786436
  7.2 14.1 %copy-start.9 = (s32[8]{0:T(128)S(1)}, s32[8]{0:T(128)}, u32[]{:S(2)}) copy-start(s32[8]{0:T(128)} %param.33) | copy-start | bytes 100
  7.2 14.1 %copy-start.7 = (f32[8,4,4]{0,2,1:T(4,128)S(1)}, f32[8,4,4]{0,2,1:T(4,128)}, u32[]{:S(2)}) copy-start(f32[8,4,4]{0,2,1:T(4,128)} %param.32) | copy-start | bytes 1540
  7.2 14.5 %copy-start.8 = (f32[8,4,4]{0,2,1:T(4,128)S(1)}, f32[8,4,4]{0,2,1:T(4,128)}, u32[]{:S(2)}) copy-start(f32[8,4,4]{0,2,1:T(4,128)} %param.31) | copy-start | bytes 1540
  7.2 14.8 %copy-start.3 = (bf16[8,4,4,128]{3,2,1,0:T(4,128)(2,1)S(1)}, bf16[8,4,4,128]{3,2,1,0:T(4,128)(2,1)}, u32[]{:S(2)}) copy-start(bf16[8,4,4,128]{3,2,1,0:T(4,128)(2,1)} %param.29) | copy-start | bytes 98308
  7.2 15.0 %copy-start.4 = (bf16[8,4,4,128]{3,2,1,0:T(4,128)(2,1)S(1)}, bf16[8,4,4,128]{3,2,1,0:T(4,128)(2,1)}, u32[]{:S(2)}) copy-start(bf16[8,4,4,128]{3,2,1,0:T(4,128)(2,1)} %param.30) | copy-start | bytes 98308
  7.2 15.1 %copy-start.2 = (f32[8,4,128,128]{3,2,1,0:T(8,128)S(1)}, f32[8,4,128,128]{3,2,1,0:T(8,128)}, u32[]{:S(2)}) copy-start(f32[8,4,128,128]{3,2,1,0:T(8,128)} %param.28) | copy-start | bytes 6291460
  7.2 146.2 %all-gather.2.cloned.1.call-start = ((), (), s32[]{:S(2)}) async-start(), calls=%async_computation.3 | async-start | bytes 17301504 | tf_op jit(solution)/shard_map/all_gather | solution.py:15
  9.4 30.2 %all-to-all-start = ((bf16[256,4,128]{2,1,0:T(4,128)(2,1)}), bf16[256,4,128]{2,1,0:T(4,128)(2,1)S(1)}, u32[]{:S(2)}, u32[]{:S(2)}) async-start(bf16[256,4,128]{2,1,0:T(4,128)(2,1)} %param.17), calls=%async_computation | async-start | bytes 524288 | tf_op jit(solution)/shard_map/all_to_all | solution.py:85
  29.8 4.0 %copy-start.10 = (f32[32]{0:T(128)S(1)}, f32[32]{0:T(128)}, u32[]{:S(2)}) copy-start(f32[32]{0:T(128)} %param.25) | copy-start | bytes 388
  39.5 154.8 %copy-start.1 = (f32[8,4,128,128]{3,2,1,0:T(8,128)}, f32[8,4,128,128]{3,2,1,0:T(8,128)S(1)}, u32[]{:S(2)}) copy-start(f32[8,4,128,128]{3,2,1,0:T(8,128)S(1)} %multiply_add_fusion.3) | copy-start | bytes 6291460
  39.6 0.7 copy-start.6
  194.3 5.6 %copy-start.11 = (f32[128]{0:T(128)S(1)}, f32[128]{0:T(128)}, u32[]{:S(2)}) copy-start(f32[128]{0:T(128)} %param.26) | copy-start | bytes 1540
  203.4 31.1 %copy-start.5 = (bf16[512,128]{1,0:T(8,128)(2,1)S(1)}, bf16[512,128]{1,0:T(8,128)(2,1)}, u32[]{:S(2)}) copy-start(bf16[512,128]{1,0:T(8,128)(2,1)} %param.27) | copy-start | bytes 393220
Sparse Core Ops, SparseCore 0:
  10.6 142.7 all-gather.1
where the time goes:
time: 260 us; the launch traced here: 259 us
  waiting for transfers between devices  110 us (42%)
  matrix products  50.4 us (19%)
  blocking collectives  47.6 us (18%)
  between operations  14.5 us (6%)
  local copies, waits for them, and re-layouts  13.9 us (5%)
  starting transfers between devices  11.9 us (5%)
  other arithmetic  10.8 us (4%)
    all_gather x1, waiting for transfers between devices, side_by_side(): lax.all_gather(both, axis, axis=dim, tiled=True)  110 us
    all_to_all x1, blocking collectives, copy_for_each(): return lax.all_to_all(copies, axis, split_axis=0, concat_axis=0, tiled=True)  30.9 us
    dot_general x8, matrix products, apply_update(): jnp.einsum('bhde,bhd->bhe', decayed, keyvec, precision=lax.Precision.HIGH...  22.1 us
    all_to_all x1, blocking collectives, summed_on_arrival(): tiles = lax.all_to_all(in_blocks(shard, dim, size), axis, 0, 0, tiled=True)  16.6 us
    dot_general x4, matrix products, per_device(): jnp.einsum('bhde,bhd->bhe', matrix, query[:, proposal], precision=lax.Pre...  14.1 us
    dot_general x4, matrix products, per_device(): jnp.dot(normed, piece, preferred_element_type=f32)  12.6 us
    all_to_all x1, starting transfers between devices, per_device(): lax.all_to_all(tokens, 'kv', split_axis=0, concat_axis=2, tiled=True)  11.9 us
    dot_general x2, local copies, waits for them, and re-layouts, per_device(): jnp.dot(normed, piece, preferred_element_type=f32)  10.8 us
  transfers between devices with their start and end apart: 2, of which 1 were waited for; matrix products, arithmetic and copies ran while one was open for 8% of the time, Pallas kernels for 0%

commit v1 on v0

v1 whole, which is shorter than its diff:
```python
import jax
import jax.numpy as jnp
from jax import lax
from jax.experimental import pallas as pl
from jax.experimental.pallas import tpu as pltpu
from jax.sharding import PartitionSpec as P

MESH = pl.DeviceIdType.MESH
HIGHEST = lax.Precision.HIGHEST
epsilon = 1e-06

NZ, NX, NY, NT, NB, NH = 8, 4, 4, 4, 8, 4
f32, bf16 = jnp.float32, jnp.bfloat16


def contract(a, b, dims, precision=None):
    return lax.dot_general(a, b, (dims, ((), ())), precision=precision, preferred_element_type=f32)


def silu(v):
    return v / (1.0 + jnp.exp(-v))


def head(h):
    return slice(h * 128, (h + 1) * 128)


def across(v):
    return jnp.sum(v, axis=-1, keepdims=True)


def delta_rule(keys, predicted, values, logs, betas):
    decay = {}
    for t in range(NT):
        total = logs[t]
        decay[t, t] = None
        for i in range(t - 1, -1, -1):
            decay[t, i] = jnp.exp(total)
            total = total + logs[i]
        decay[t, -1] = jnp.exp(total)
    written = []
    for t in range(NT):
        expected = decay[t, -1] * predicted[t]
        for i in range(t):
            expected = expected + decay[t, i] * across(keys[i] * keys[t]) * written[i]
        written.append(betas[t] * (values[t] - expected))
    return written, decay


def kernel(
    tok, wkey, wquery, wvalue, wgate, wout, state, gain, abw, kold, vold, gold, bold, rate, hgain,
    mixed, carried,
    xtok, wbuf, stsend, strecv, scol, nbuf, absend, abrecv, yown, y1send, y1recv, y2send, y2recv,
    wobuf, sbuf, pbuf, ubuf, ebuf, tmp, kq, gnew, bnew, vnew, hout, hsend, hz, p3, d2d, rs2, yrecv, ofin, orecv,
    loc, ts, tr, wds, wdr, wrs, wrr, sts, str_, abs_, abr, y1s, y1r, y2s, y2r, wos, wor, hs, hr, ds_, dr, ys, yr, os_, or_,
):
    kv, tp = lax.axis_index("kv"), lax.axis_index("tp")
    z, x, y, c = kv // NX, lax.rem(kv, NX), tp // 2, lax.rem(tp, 2)
    side = 2 * lax.rem(z, 2) - 1
    weights = (wkey, wquery, wvalue, wgate)

    def at_z(zz):
        return {"kv": lax.rem(zz + 2 * NZ, NZ) * NX + x}

    def at_x(xx):
        return {"kv": z * NX + lax.rem(xx + NX, NX)}

    def at_y(yy):
        return {"tp": lax.rem(yy + NY, NY) * 2 + c}

    def dest(r):
        off = side * r if r < 4 else -side * (r - 3)
        return lax.rem(z + off + 2 * NZ, NZ)

    def remote(src, dst, send, recv, device):
        return pltpu.make_async_remote_copy(
            src_ref=src, dst_ref=dst, send_sem=send, recv_sem=recv, device_id=device, device_id_type=MESH
        )

    twin = {"tp": tp + 1 - 2 * c}
    pending = []

    def go(copy):
        copy.start()
        pending.append(copy)
        return copy

    own_tok = pltpu.make_async_copy(tok.at[:, x], xtok.at[0], loc.at[0])
    own_tok.start()
    own_w = [pltpu.make_async_copy(weights[m], wbuf.at[m, 0], loc.at[1 + m]) for m in range(4)]
    for copy in own_w:
        copy.start()
    own_s = pltpu.make_async_copy(state, sbuf, loc.at[5])
    own_s.start()
    own_wo = pltpu.make_async_copy(wout, wobuf.at[:, pl.ds(0, 128)], loc.at[6])
    own_wo.start()

    barrier = pltpu.get_barrier_semaphore()
    for d in range(1, NX):
        pl.semaphore_signal(barrier, inc=1, device_id=at_x(x + d), device_id_type=MESH)
    for d in range(1, NZ):
        pl.semaphore_signal(barrier, inc=1, device_id=at_z(z + d), device_id_type=MESH)
    for d in range(1, NY):
        pl.semaphore_signal(barrier, inc=1, device_id=at_y(y + d), device_id_type=MESH)
    pl.semaphore_signal(barrier, inc=1, device_id=twin, device_id_type=MESH)
    pl.semaphore_wait(barrier, NX + NZ + NY - 2)

    toks = [
        go(remote(tok.at[:, lax.rem(x + d, NX)], xtok.at[d], ts.at[d - 1], tr.at[d - 1], at_x(x + d)))
        for d in range(1, NX)
    ]

    def direct(m):
        return [
            go(remote(weights[m], wbuf.at[m, 1], wds.at[m, 0], wdr.at[m, 0], at_x(x + 1))),
            go(remote(weights[m], wbuf.at[m, 3], wds.at[m, 1], wdr.at[m, 1], at_x(x + 3))),
        ]

    def relay(m, copies):
        low, high = pl.ds(0, 64), pl.ds(64, 64)
        copies[0].wait_recv()
        first = go(remote(wbuf.at[m, 1, low], wbuf.at[m, 2, low], wrs.at[m, 0], wrr.at[m, 0], at_x(x + 1)))
        copies[1].wait_recv()
        second = go(remote(wbuf.at[m, 3, high], wbuf.at[m, 2, high], wrs.at[m, 1], wrr.at[m, 1], at_x(x + 3)))
        return [first, second]

    d0 = direct(0)
    d1 = direct(1)

    own_tok.wait()
    for copy in toks:
        copy.wait_recv()
    squares = jnp.zeros((NZ * 32, 128), f32)
    for d in range(NX):
        part = xtok[d].reshape(NZ * 32, 128).astype(f32)
        squares = squares + part * part
    stsend[...] = contract(jnp.ones((8, 128), f32), squares, ((1,), (1,)), HIGHEST)
    stats = [
        go(remote(stsend, strecv.at[d - 1], sts.at[d - 1], str_.at[d - 1], at_z(z + d))) for d in range(1, NZ)
    ]

    def products(left, b, h):
        rows = pl.ds(pl.multiple_of(b * 8, 8), 8)
        pbuf[h, rows] = contract(left[h, rows], sbuf[b * NH + h], ((1,), (0,)), HIGHEST)

    def all_products(left):
        @pl.loop(0, NB)
        def _(b):
            for h in range(NH):
                products(left, b, h)

    def every(ref, start, h):
        return ref[h, pl.ds(start, 8, stride=8)]

    own_s.wait()
    all_products(kold)

    r0 = relay(0, d0)
    d2 = direct(2)

    for copy in stats:
        copy.wait_recv()
    total = stsend[...]
    for d in range(NZ - 1):
        total = total + strecv[d]
    scale = lax.rsqrt(total * (1.0 / (NX * NZ * 128)) + epsilon)
    first_row = (lax.broadcasted_iota(jnp.int32, (8, 128), 0) == 0).astype(f32)
    scol[...] = contract(scale, first_row, ((0,), (0,)), HIGHEST).reshape(NZ, 32, 128)
    absend[...] = jnp.zeros((NZ, 8, 128), f32)
    for r in range(NZ):
        zz = dest(r)
        small = jnp.zeros((16, 32), f32)
        for d in range(NX):
            feature = lax.rem(x + NX - d, NX)
            normed = (xtok[d, zz].astype(f32) * scol[zz] * gain[feature]).astype(bf16)
            nbuf[r * 32 : (r + 1) * 32, head(d)] = normed
            small = small + contract(abw[feature], normed, ((1,), (1,)))
        absend[r, :, 0:32] = small[0:8]
    ab = [
        go(remote(absend.at[r], abrecv.at[r - 1], abs_.at[r - 1], abr.at[r - 1], at_z(dest(r))))
        for r in range(1, NZ)
    ]

    def project(m, copies):
        own_w[m].wait()
        for copy in copies:
            copy.wait_recv()
        rows = jnp.dot(nbuf[...], wbuf[m].reshape(512, 512), preferred_element_type=f32)
        yown[m] = rows[0:128]
        y1send[m] = rows[128:256].astype(bf16)
        return go(remote(y1send.at[m], y1recv.at[m], y1s.at[m], y1r.at[m], at_z(z + (-side))))

    def second_sum(m, copy):
        copy.wait_recv()
        rows = yown[m] + y1recv[m].astype(f32)
        yown[m, 0:32] = rows[0:32]
        y2send[m] = rows[32:128].astype(bf16).reshape(3, 32, 512)
        return [
            go(remote(y2send.at[m, i - 1], y2recv.at[m, i - 1], y2s.at[m, i - 1], y2r.at[m, i - 1], at_z(dest(i))))
            for i in (3, 2, 1)
        ]

    def summed(m, copies, lanes):
        rows = yown[m, 0:32, lanes]
        for i in range(3):
            rows = rows + y2recv[m, i, :, lanes].astype(f32)
        return rows

    y1_0 = project(0, r0)
    r1 = relay(1, d1)
    d3 = direct(3)

    for h in range(NH):
        keys = [every(kold, t, h) for t in range(NT)]
        written, decay = delta_rule(
            keys,
            [every(pbuf, t, h) for t in range(NT)],
            [vold[t, :, head(h)] for t in range(NT)],
            [gold[t, :, head(h)] for t in range(NT)],
            [bold[t, :, head(h)] for t in range(NT)],
        )
        for t in range(NT):
            last = written[t] if t == NT - 1 else decay[NT - 1, t] * written[t]
            ubuf[h, pl.ds(t, 8, stride=8)] = last
            ubuf[h, pl.ds(t + 4, 8, stride=8)] = jnp.zeros((8, 128), f32)
        ebuf[h, pl.ds(0, 8, stride=8)] = decay[NT - 1, -1]

    y2_0 = second_sum(0, y1_0)
    y1_1 = project(1, r1)
    r2 = relay(2, d2)
    wos_ = [
        go(remote(wout, wobuf.at[:, pl.ds(d * 128, 128)], wos.at[d - 1], wor.at[d - 1], at_x(x + d)))
        for d in range(1, NX)
    ]

    @pl.loop(0, NB)
    def _(b):
        rows = pl.ds(pl.multiple_of(b * 8, 8), 8)
        for h in range(NH):
            added = contract(kold[h, rows], ubuf[h, rows], ((0,), (0,)), HIGHEST)
            sbuf[b * NH + h] = sbuf[b * NH + h] * ebuf[h, rows][0:1] + added

    out_s = pltpu.make_async_copy(sbuf, carried, loc.at[7])
    out_s.start()

    y2_1 = second_sum(1, y1_1)
    y1_2 = project(2, r2)
    r3 = relay(3, d3)

    for copy in ab:
        copy.wait_recv()
    small = absend[0]
    for r in range(NZ - 1):
        small = small + abrecv[r]
    soft = jnp.maximum(small, 0.0) + jnp.log1p(jnp.exp(-jnp.abs(small)))
    which = lax.broadcasted_iota(jnp.int32, (8, 128), 0)
    small = jnp.where(which < NH, -rate[...] * soft, 1.0 / (1.0 + jnp.exp(-small)))
    row = lax.broadcasted_iota(jnp.int32, (8, 512), 0)
    lane = lax.broadcasted_iota(jnp.int32, (8, 512), 1) // 128
    logs = contract(small, (row == lane).astype(f32), ((0,), (0,)), HIGHEST)
    strengths = contract(small, (row == lane + NH).astype(f32), ((0,), (0,)), HIGHEST)
    for h in range(NH):
        gnew[h] = logs[0:32, head(h)]
        bnew[h] = strengths[0:32, head(h)]

    y1_3 = project(3, r3)
    y2_2 = second_sum(2, y1_2)

    def rows_of(ref, t, h):
        return ref[h, pl.ds(t, 8, stride=4)]

    for m, copies, factor in ((0, y2_0, 1.0), (1, y2_1, 128**-0.5)):
        for copy in copies:
            copy.wait_recv()
        for h in range(NH):
            v = silu(summed(m, copies, head(h)))
            tmp[h] = v * lax.rsqrt(across(v * v) + epsilon) * factor
            for t in range(NT):
                kq[h, pl.ds(m * 4 + t, 8, stride=8)] = rows_of(tmp, t, h)
    all_products(kq)

    y2_3 = second_sum(3, y1_3)
    for copy in y2_2:
        copy.wait_recv()
    for h in range(NH):
        vnew[h] = silu(summed(2, y2_2, head(h)))
    for h in range(NH):
        keys = [every(kq, t, h) for t in range(NT)]
        written, decay = delta_rule(
            keys,
            [every(pbuf, t, h) for t in range(NT)],
            [rows_of(vnew, t, h) for t in range(NT)],
            [rows_of(gnew, t, h) for t in range(NT)],
            [rows_of(bnew, t, h) for t in range(NT)],
        )
        for t in range(NT):
            query = every(kq, 4 + t, h)
            attended = decay[t, -1] * every(pbuf, 4 + t, h) + across(keys[t] * query) * written[t]
            for i in range(t):
                attended = attended + decay[t, i] * across(keys[i] * query) * written[i]
            scaled = attended * lax.rsqrt(across(attended * attended) * (1.0 / 128) + epsilon)
            hout[h, pl.ds(t, 8, stride=4)] = scaled * hgain[...]

    for copy in y2_3:
        copy.wait_recv()
    for h in range(NH):
        hsend[:, head(h)] = (hout[h] * silu(summed(3, y2_3, head(h)))).astype(bf16)
    heads = [go(remote(hsend, hz.at[d], hs.at[d - 1], hr.at[d - 1], at_z(z + d))) for d in (4, 3, 5, 2, 6, 1, 7)]
    hz[0] = hsend[...]

    own_wo.wait()
    for copy in wos_:
        copy.wait_recv()
    for copy in heads:
        copy.wait_recv()
    terms = jnp.dot(hz[...].reshape(256, 512), wobuf[...], preferred_element_type=f32)
    for d in range(NZ):
        zz = lax.rem(z + NZ - d, NZ)
        p3[lax.rem(zz, 2) * 4 + zz // 2] = terms[d * 32 : (d + 1) * 32]
    other = go(remote(p3.at[pl.ds((1 - c) * 4, 4)], d2d, ds_, dr, twin))
    other.wait_recv()
    for j in range(NY):
        rs2[j] = p3[c * 4 + j] + d2d[j]
    across_y = [
        go(remote(rs2.at[lax.rem(y + e, NY)], yrecv.at[e - 1], ys.at[e - 1], yr.at[e - 1], at_y(y + e)))
        for e in (2, 1, 3)
    ]
    for copy in across_y:
        copy.wait_recv()
    total = rs2[y]
    for e in range(NY - 1):
        total = total + yrecv[e]
    total = total.astype(bf16)
    for e in range(NX):
        ofin[e] = total[:, head(e)]
    outs = [
        go(remote(ofin.at[e], orecv.at[e - 1], os_.at[e - 1], or_.at[e - 1], at_x(x + NX - e)))
        for e in range(1, NX)
    ]
    mixed[x] = ofin[0]
    for e in range(1, NX):
        outs[e - 1].wait_recv()
        mixed[lax.rem(x + e, NX)] = orecv[e - 1]
    out_s.wait()
    for copy in pending:
        copy.wait_send()


def fused(*operands):
    anywhere = pl.BlockSpec(memory_space=pl.ANY)
    vmem = pl.BlockSpec(memory_space=pltpu.VMEM)
    dma = pltpu.SemaphoreType.DMA
    scratch = [
        pltpu.VMEM((NX, NZ, 32, 128), bf16),
        pltpu.VMEM((4, NX, 128, 512), bf16),
        pltpu.VMEM((8, 256), f32),
        pltpu.VMEM((NZ - 1, 8, 256), f32),
        pltpu.VMEM((NZ, 32, 128), f32),
        pltpu.VMEM((256, 512), bf16),
        pltpu.VMEM((NZ, 8, 128), f32),
        pltpu.VMEM((NZ - 1, 8, 128), f32),
        pltpu.VMEM((4, 128, 512), f32),
        pltpu.VMEM((4, 128, 512), bf16),
        pltpu.VMEM((4, 128, 512), bf16),
        pltpu.VMEM((4, 3, 32, 512), bf16),
        pltpu.VMEM((4, 3, 32, 512), bf16),
        pltpu.VMEM((512, 512), bf16),
        pltpu.VMEM((NB * NH, 128, 128), f32),
        pltpu.VMEM((NH, 64, 128), f32),
        pltpu.VMEM((NH, 64, 128), f32),
        pltpu.VMEM((NH, 64, 128), f32),
        pltpu.VMEM((NH, 32, 128), f32),
        pltpu.VMEM((NH, 64, 128), f32),
        pltpu.VMEM((NH, 32, 128), f32),
        pltpu.VMEM((NH, 32, 128), f32),
        pltpu.VMEM((NH, 32, 128), f32),
        pltpu.VMEM((NH, 32, 128), f32),
        pltpu.VMEM((32, 512), bf16),
        pltpu.VMEM((NZ, 32, 512), bf16),
        pltpu.VMEM((NZ, 32, 512), f32),
        pltpu.VMEM((NY, 32, 512), f32),
        pltpu.VMEM((NY, 32, 512), f32),
        pltpu.VMEM((NY - 1, 32, 512), f32),
        pltpu.VMEM((NX, 32, 128), bf16),
        pltpu.VMEM((NX - 1, 32, 128), bf16),
        dma((8,)),
        dma((3,)), dma((3,)),
        dma((4, 2)), dma((4, 2)), dma((4, 2)), dma((4, 2)),
        dma((7,)), dma((7,)), dma((7,)), dma((7,)),
        dma((4,)), dma((4,)), dma((4, 3)), dma((4, 3)),
        dma((3,)), dma((3,)),
        dma((7,)), dma((7,)),
        dma, dma,
        dma((3,)), dma((3,)), dma((3,)), dma((3,)),
    ]
    return pl.pallas_call(
        kernel,
        out_shape=(
            jax.ShapeDtypeStruct((NX, 32, 128), bf16),
            jax.ShapeDtypeStruct((NB * NH, 128, 128), f32),
        ),
        in_specs=[anywhere] * 7 + [vmem] * 8,
        out_specs=(vmem, anywhere),
        scratch_shapes=scratch,
        compiler_params=pltpu.CompilerParams(collective_id=0, has_side_effects=True),
        name="step",
    )(*operands)


def unit_rows(values):
    return values * lax.rsqrt(jnp.sum(values * values, axis=-1, keepdims=True) + epsilon)


def per_device(
    tokens,
    norm_gain,
    w_query,
    w_key,
    w_value,
    w_gate,
    w_decay,
    w_beta,
    decay_rate,
    head_gain,
    w_out,
    state,
    prev_keys,
    prev_values,
    prev_log_decay,
    prev_beta,
    accepted,
):
    z = lax.axis_index("kv") // NX
    head_start = lax.axis_index("tp") * NH
    gain = lax.dynamic_slice_in_dim(norm_gain, z * 512, 512, 0).reshape(NX, 1, 128)
    both = [lax.dynamic_slice(w, (z * 512, head_start), (512, NH)).T for w in (w_decay, w_beta)]
    abw = jnp.concatenate(both + [jnp.zeros((8, 512), bf16)], axis=0)
    abw = abw.reshape(16, NX, 128).transpose(1, 0, 2)
    rate = jnp.pad(lax.dynamic_slice_in_dim(decay_rate, head_start, NH, 0), (0, 4))
    rate = jnp.broadcast_to(rate[:, None], (8, 128))

    def by_step(v):
        return v.transpose(2, 0, 1, 3).reshape(NT, NB, NH * 128)

    kold = unit_rows(prev_keys.astype(f32)).transpose(1, 0, 2, 3)
    kold = jnp.pad(kold, ((0, 0), (0, 0), (0, 4), (0, 0))).reshape(NH, NB * 8, 128)
    vold = by_step(prev_values.astype(f32))
    keep = (jnp.arange(NT)[None, :] < accepted[:, None]).astype(f32)[:, None, :]
    wide = (NB, NH, NT, 128)
    gold = by_step(jnp.broadcast_to((prev_log_decay * keep)[..., None], wide))
    bold = by_step(jnp.broadcast_to((prev_beta * keep)[..., None], wide))
    mixed, carried = fused(
        tokens.reshape(NZ, NX, 32, 128), w_key, w_query, w_value, w_gate, w_out,
        state.reshape(NB * NH, 128, 128), gain, abw, kold, vold, gold, bold, rate, head_gain.reshape(1, 128),
    )
    return mixed.reshape(32, NT, 128), carried.reshape(NB, NH, 128, 128)


def solution(mesh):
    placed = (
        P(None, None, "kv"),
        P(),
        P("kv", "tp"),
        P("kv", "tp"),
        P("kv", "tp"),
        P("kv", "tp"),
        P(),
        P(),
        P(),
        P(),
        P("tp", "kv"),
        P("kv", "tp", None, None),
        P("kv", "tp", None, None),
        P("kv", "tp", None, None),
        P("kv", "tp", None),
        P("kv", "tp", None),
        P("kv"),
    )
    return jax.shard_map(
        per_device,
        mesh=mesh,
        in_specs=placed,
        out_specs=(P("tp", None, "kv"), P("kv", "tp", None, None)),
        check_vma=False,
    )
```

time: 260 us -> 85.9 us (0.33)
  waiting for transfers between devices: 110 us -> 0 us
  Pallas kernels: 0 us -> 69.9 us
  matrix products: 50.4 us -> 0 us
  blocking collectives: 47.6 us -> 0 us
  between operations: 14.5 us -> 0.68 us
  starting transfers between devices: 11.9 us -> 0 us
  other arithmetic: 10.8 us -> 5.22 us
  local copies, waits for them, and re-layouts: 13.9 us -> 9.55 us
    all_gather x1 -> x0, waiting for transfers between devices: 110 us -> none  [side_by_side(): lax.all_gather(both, axis, axis=dim, tiled=True)]
    pallas_call x0 -> x1, Pallas kernels: none -> 69.9 us  [fused(): pl.pallas_call(kernel, out_shape=(jax.ShapeDtypeStruct((NX, 32, 128), bf1...]
    dot_general x19 -> x0, matrix products: 50.4 us -> none  [the longest x8 22.1 us: apply_update(): jnp.einsum('bhde,bhd->bhe', decayed, keyvec, precision=lax.Precision.HIGH...]
    all_to_all x2 -> x0, blocking collectives: 47.6 us -> none  [the longest x1 30.9 us: copy_for_each(): return lax.all_to_all(copies, axis, split_axis=0, concat_axis=0, tiled=True)]
    all_to_all x1 -> x0, starting transfers between devices: 11.9 us -> none  [per_device(): lax.all_to_all(tokens, 'kv', split_axis=0, concat_axis=2, tiled=True)]
    dot_general x6 -> x0, local copies, waits for them, and re-layouts: 10.9 us -> none  [the longest x2 10.8 us: per_device(): jnp.dot(normed, piece, preferred_element_type=f32)]
    add x1 -> x0, other arithmetic: 5.69 us -> none  [apply_update(): decayed + jnp.einsum('bhd,bhe->bhde', keyvec, change, precision=lax.Preci...]
    unnamed x25 -> x3, local copies, waits for them, and re-layouts: 0.1 us -> 4.52 us
  transfers between devices with their start and end apart: 2 -> 0, of which waited for: 1 -> 0; matrix products, arithmetic and copies ran while one was open for 8% -> 0% of each run, Pallas kernels for 0% -> 0%
where the time goes in v1:
time: 85.9 us; the launch traced here: 85.4 us
  Pallas kernels  69.9 us (81%)
  local copies, waits for them, and re-layouts  9.55 us (11%)
  other arithmetic  5.22 us (6%)
    pallas_call x1, Pallas kernels, fused(): pl.pallas_call(kernel, out_shape=(jax.ShapeDtypeStruct((NX, 32, 128), bf1...  69.9 us
    unnamed x3, local copies, waits for them, and re-layouts  4.52 us

profile of v1, /device:TPU:1, one launch (start us, length us, event | category | flops | bytes accessed | tf_op | source)
XLA Modules:
  0.0 85.4 jit_solution(14450798932442451906)
XLA Ops:
  0.7 0.7 dynamic_slice.15
  1.4 0.1 pad.12.clone
  1.5 1.3 %dynamic_slice.12 = f32[512]{0:T(512)} dynamic-slice(f32[4096]{0:T(1024)} %param.18, s32[]{:T(128)S(6)} %select_n.16), dynamic_slice_sizes={512} | dynamic-slice | bytes 4100 | tf_op jit(solution)/shard_map/dynamic_slice | solution.py:435
  2.8 0.7 fusion.2
  3.5 0.7 broadcast_in_dim.11.rate
  4.1 0.8 dynamic-slice_bitcast_fusion
  4.9 0.7 bitcast_bitcast_fusion.abw
  5.6 0.7 broadcast_multiply_fusion
  6.3 0.9 %fusion = f32[8,4,4]{2,1,0:T(4,128)S(1)} fusion(bf16[8,4,4,128]{3,2,1,0:T(4,128)(2,1)} %param.29), kind=kLoop, calls=%fused_computation.3 | loop fusion | flops 49024 | bytes 33280 | tf_op jit(solution)/shard_map/reduce_sum | solution.py:411
  7.2 0.8 convert_bitcast_fusion
  8.0 0.6 copy.34
  8.7 1.5 %pad_bitcast_fusion.kold = f32[4,64,128]{2,1,0:T(8,128)} fusion(bf16[8,4,4,128]{3,2,1,0:T(4,128)(2,1)} %param.29, f32[8,4,4]{2,1,0:T(4,128)S(1)} %add_rsqrt_fusion), kind=kLoop, calls=%fused_computation | loop fusion | flops 32768 | bytes 164352 | tf_op jit(solution)/shard_map/reshape | solution.py:446
  10.2 0.8 broadcast_bitcast_fusion
  10.9 69.9 %step.1 = (bf16[4,32,128]{2,1,0:T(8,128)(2,1)}, f32[32,128,128]{2,1,0:T(8,128)}) custom-call(bf16[8,4,32,128]{3,2,1,0:T(8,128)(2,1)} %bitcast.43, bf16[128,512]{1,0:T(8,128)(2,1)} %wkey.1, bf16[128,512]{1,0:T(8,128)(2,1)} %wquery.1, bf16[128,512]{1,0:T(8,128)(2,1)} %wvalue.1, bf16[128,512]{1,0:T(8,128)(2,1)} %wgate.1, bf16[512,128]{1,0:T(8,128)(2,1)} %wout.1, ...), custom_call_target="tpu_custom_call" | custom-call | tf_op jit(solution)/shard_map/step/pallas_call | solution.py:396
  80.9 1.4 %copy.37 = bf16[32,4,128]{2,1,0:T(4,128)(2,1)} copy(bf16[32,4,128]{2,1,0:T(4,128)(2,1)} %bitcast.45) | data formatting | bytes 65536
  82.3 3.1 %copy.38 = f32[8,4,128,128]{3,2,1,0:T(8,128)} copy(f32[8,4,128,128]{3,2,1,0:T(8,128)} %bitcast.42) | data formatting | bytes 4194304
  (6 shorter events, 0.0 us)

commit v2 on v1

--- a/solution.py
+++ b/solution.py
@@ -48,12 +48,16 @@
 
 
 def kernel(
-    tok, wkey, wquery, wvalue, wgate, wout, state, gain, abw, kold, vold, gold, bold, rate, hgain,
-    mixed, carried,
-    xtok, wbuf, stsend, strecv, scol, nbuf, absend, abrecv, yown, y1send, y1recv, y2send, y2recv,
-    wobuf, sbuf, pbuf, ubuf, ebuf, tmp, kq, gnew, bnew, vnew, hout, hsend, hz, p3, d2d, rs2, yrecv, ofin, orecv,
+    tok, wkey, wquery, wvalue, wgate, wout, state, *rest
+):
+    small_in, (mixed, sbuf, *rest) = rest[:10], rest[10:]
+    small_ref, rest = rest[:10], rest[10:]
+    gain, wdecay, wbeta, pkeys, pvalues, plogs, pbetas, accepted, rate, hgain = small_ref
+    (
+    small_sem, kraw, vraw, kold, gold, bold, abw, gainrow, xtok, wbuf, stsend, strecv, scol, nbuf, absend, abrecv, yown, y1send, y1recv, y2send, y2recv,
+    wobuf, pbuf, ubuf, ebuf, tmp, kq, gnew, bnew, vnew, hout, hsend, hz, p3, d2d, rs2, yrecv, ofin, orecv,
     loc, ts, tr, wds, wdr, wrs, wrr, sts, str_, abs_, abr, y1s, y1r, y2s, y2r, wos, wor, hs, hr, ds_, dr, ys, yr, os_, or_,
-):
+    ) = rest
     kv, tp = lax.axis_index("kv"), lax.axis_index("tp")
     z, x, y, c = kv // NX, lax.rem(kv, NX), tp // 2, lax.rem(tp, 2)
     side = 2 * lax.rem(z, 2) - 1
@@ -84,6 +88,11 @@
         copy.start()
         pending.append(copy)
         return copy
+
+    def arrive(name, *copies):
+        with jax.named_scope(name):
+            for copy in copies:
+                copy.wait_recv()
 
     own_tok = pltpu.make_async_copy(tok.at[:, x], xtok.at[0], loc.at[0])
     own_tok.start()
@@ -92,6 +101,12 @@
         copy.start()
     own_s = pltpu.make_async_copy(state, sbuf, loc.at[5])
     own_s.start()
+    sources = list(small_in)
+    for i in (1, 2):
+        sources[i] = small_in[i].at[:, pl.ds(pl.multiple_of(z * 512, 512), 512)]
+    own_small = [pltpu.make_async_copy(a, b, small_sem.at[i]) for i, (a, b) in enumerate(zip(sources, small_ref))]
+    for copy in own_small:
+        copy.start()
     own_wo = pltpu.make_async_copy(wout, wobuf.at[:, pl.ds(0, 128)], loc.at[6])
     own_wo.start()
 
@@ -103,7 +118,8 @@
     for d in range(1, NY):
         pl.semaphore_signal(barrier, inc=1, device_id=at_y(y + d), device_id_type=MESH)
     pl.semaphore_signal(barrier, inc=1, device_id=twin, device_id_type=MESH)
-    pl.semaphore_wait(barrier, NX + NZ + NY - 2)
+    with jax.named_scope("barrier"):
+        pl.semaphore_wait(barrier, NX + NZ + NY - 2)
 
     toks = [
         go(remote(tok.at[:, lax.rem(x + d, NX)], xtok.at[d], ts.at[d - 1], tr.at[d - 1], at_x(x + d)))
@@ -118,18 +134,42 @@
 
     def relay(m, copies):
         low, high = pl.ds(0, 64), pl.ds(64, 64)
-        copies[0].wait_recv()
+        arrive(f"left{m}", copies[0])
         first = go(remote(wbuf.at[m, 1, low], wbuf.at[m, 2, low], wrs.at[m, 0], wrr.at[m, 0], at_x(x + 1)))
-        copies[1].wait_recv()
+        arrive(f"right{m}", copies[1])
         second = go(remote(wbuf.at[m, 3, high], wbuf.at[m, 2, high], wrs.at[m, 1], wrr.at[m, 1], at_x(x + 3)))
         return [first, second]
 
     d0 = direct(0)
     d1 = direct(1)
 
+    for copy in own_small:
+        copy.wait()
+    row = lax.broadcasted_iota(jnp.int32, (16, 32), 0)
+    col = lax.broadcasted_iota(jnp.int32, (16, 32), 1) - tp * NH
+    abw[...] = (
+        contract(((row == col) & (row < NH)).astype(bf16), wdecay[...], ((1,), (0,)))
+        + contract(((row == col + NH) & (row >= NH) & (row < 2 * NH)).astype(bf16), wbeta[...], ((1,), (0,)))
+    ).astype(bf16)
+    row = lax.broadcasted_iota(jnp.int32, (NX * NZ, 128), 0)
+    for d in range(NX):
+        here = row == z * NX + lax.rem(x + NX - d, NX)
+        gainrow[d] = jnp.sum(jnp.where(here, gain[...], 0.0), axis=0, keepdims=True)
+    keys = pkeys[...].astype(f32)
+    kraw[...] = keys * lax.rsqrt(across(keys * keys) + epsilon)
+    vraw[...] = pvalues[...].astype(f32)
+    for h in range(NH):
+        for t in range(NT):
+            kold[h, pl.ds(t, 8, stride=8)] = kraw[pl.ds(h * NT + t, 8, stride=16)]
+            kold[h, pl.ds(t + 4, 8, stride=8)] = jnp.zeros((8, 128), f32)
+    kept = lax.rem(lax.broadcasted_iota(jnp.int32, (16, 8), 0), NT) < accepted[...]
+    spread = lax.broadcasted_iota(jnp.int32, (16, 2048), 0) == lax.broadcasted_iota(jnp.int32, (16, 2048), 1) // 128
+    spread = spread.astype(f32)
+    gold[...] = contract(jnp.where(kept, plogs[...], 0.0), spread, ((0,), (0,)), HIGHEST)
+    bold[...] = contract(jnp.where(kept, pbetas[...], 0.0), spread, ((0,), (0,)), HIGHEST)
+
     own_tok.wait()
-    for copy in toks:
-        copy.wait_recv()
+    arrive("tokens", *toks)
     squares = jnp.zeros((NZ * 32, 128), f32)
     for d in range(NX):
         part = xtok[d].reshape(NZ * 32, 128).astype(f32)
@@ -158,8 +198,7 @@
     r0 = relay(0, d0)
     d2 = direct(2)
 
-    for copy in stats:
-        copy.wait_recv()
+    arrive("stats", *stats)
     total = stsend[...]
     for d in range(NZ - 1):
         total = total + strecv[d]
@@ -172,9 +211,9 @@
         small = jnp.zeros((16, 32), f32)
         for d in range(NX):
             feature = lax.rem(x + NX - d, NX)
-            normed = (xtok[d, zz].astype(f32) * scol[zz] * gain[feature]).astype(bf16)
+            normed = (xtok[d, zz].astype(f32) * scol[zz] * gainrow[d]).astype(bf16)
             nbuf[r * 32 : (r + 1) * 32, head(d)] = normed
-            small = small + contract(abw[feature], normed, ((1,), (1,)))
+            small = small + contract(abw[:, pl.ds(pl.multiple_of(feature * 128, 128), 128)], normed, ((1,), (1,)))
         absend[r, :, 0:32] = small[0:8]
     ab = [
         go(remote(absend.at[r], abrecv.at[r - 1], abs_.at[r - 1], abr.at[r - 1], at_z(dest(r))))
@@ -183,15 +222,14 @@
 
     def project(m, copies):
         own_w[m].wait()
-        for copy in copies:
-            copy.wait_recv()
+        arrive(f"far{m}", *copies)
         rows = jnp.dot(nbuf[...], wbuf[m].reshape(512, 512), preferred_element_type=f32)
         yown[m] = rows[0:128]
         y1send[m] = rows[128:256].astype(bf16)
         return go(remote(y1send.at[m], y1recv.at[m], y1s.at[m], y1r.at[m], at_z(z + (-side))))
 
     def second_sum(m, copy):
-        copy.wait_recv()
+        arrive(f"pair{m}", copy)
         rows = yown[m] + y1recv[m].astype(f32)
         yown[m, 0:32] = rows[0:32]
         y2send[m] = rows[32:128].astype(bf16).reshape(3, 32, 512)
@@ -215,9 +253,9 @@
         written, decay = delta_rule(
             keys,
             [every(pbuf, t, h) for t in range(NT)],
-            [vold[t, :, head(h)] for t in range(NT)],
-            [gold[t, :, head(h)] for t in range(NT)],
-            [bold[t, :, head(h)] for t in range(NT)],
+            [vraw[pl.ds(h * NT + t, 8, stride=16)] for t in range(NT)],
+            [gold[:, head(h * NT + t)] for t in range(NT)],
+            [bold[:, head(h * NT + t)] for t in range(NT)],
         )
         for t in range(NT):
             last = written[t] if t == NT - 1 else decay[NT - 1, t] * written[t]
@@ -240,21 +278,20 @@
             added = contract(kold[h, rows], ubuf[h, rows], ((0,), (0,)), HIGHEST)
             sbuf[b * NH + h] = sbuf[b * NH + h] * ebuf[h, rows][0:1] + added
 
-    out_s = pltpu.make_async_copy(sbuf, carried, loc.at[7])
-    out_s.start()
-
     y2_1 = second_sum(1, y1_1)
     y1_2 = project(2, r2)
     r3 = relay(3, d3)
 
-    for copy in ab:
-        copy.wait_recv()
+    arrive("small", *ab)
     small = absend[0]
     for r in range(NZ - 1):
         small = small + abrecv[r]
     soft = jnp.maximum(small, 0.0) + jnp.log1p(jnp.exp(-jnp.abs(small)))
     which = lax.broadcasted_iota(jnp.int32, (8, 128), 0)
-    small = jnp.where(which < NH, -rate[...] * soft, 1.0 / (1.0 + jnp.exp(-small)))
+    lane = lax.broadcasted_iota(jnp.int32, (8, 32), 1)
+    mine = lane == tp * NH + lax.broadcasted_iota(jnp.int32, (8, 32), 0)
+    rates = jnp.sum(jnp.where(mine, rate[...], 0.0), axis=1, keepdims=True)
+    small = jnp.where(which < NH, -rates * soft, 1.0 / (1.0 + jnp.exp(-small)))
     row = lax.broadcasted_iota(jnp.int32, (8, 512), 0)
     lane = lax.broadcasted_iota(jnp.int32, (8, 512), 1) // 128
     logs = contract(small, (row == lane).astype(f32), ((0,), (0,)), HIGHEST)
@@ -270,8 +307,7 @@
         return ref[h, pl.ds(t, 8, stride=4)]
 
     for m, copies, factor in ((0, y2_0, 1.0), (1, y2_1, 128**-0.5)):
-        for copy in copies:
-            copy.wait_recv()
+        arrive(f"sum{m}", *copies)
         for h in range(NH):
             v = silu(summed(m, copies, head(h)))
             tmp[h] = v * lax.rsqrt(across(v * v) + epsilon) * factor
@@ -280,8 +316,7 @@
     all_products(kq)
 
     y2_3 = second_sum(3, y1_3)
-    for copy in y2_2:
-        copy.wait_recv()
+    arrive("sum2", *y2_2)
     for h in range(NH):
         vnew[h] = silu(summed(2, y2_2, head(h)))
     for h in range(NH):
@@ -301,32 +336,28 @@
             scaled = attended * lax.rsqrt(across(attended * attended) * (1.0 / 128) + epsilon)
             hout[h, pl.ds(t, 8, stride=4)] = scaled * hgain[...]
 
-    for copy in y2_3:
-        copy.wait_recv()
+    arrive("sum3", *y2_3)
     for h in range(NH):
         hsend[:, head(h)] = (hout[h] * silu(summed(3, y2_3, head(h)))).astype(bf16)
     heads = [go(remote(hsend, hz.at[d], hs.at[d - 1], hr.at[d - 1], at_z(z + d))) for d in (4, 3, 5, 2, 6, 1, 7)]
     hz[0] = hsend[...]
 
     own_wo.wait()
-    for copy in wos_:
-        copy.wait_recv()
-    for copy in heads:
-        copy.wait_recv()
+    arrive("wout", *wos_)
+    arrive("heads", *heads)
     terms = jnp.dot(hz[...].reshape(256, 512), wobuf[...], preferred_element_type=f32)
     for d in range(NZ):
         zz = lax.rem(z + NZ - d, NZ)
         p3[lax.rem(zz, 2) * 4 + zz // 2] = terms[d * 32 : (d + 1) * 32]
     other = go(remote(p3.at[pl.ds((1 - c) * 4, 4)], d2d, ds_, dr, twin))
-    other.wait_recv()
+    arrive("twin", other)
     for j in range(NY):
         rs2[j] = p3[c * 4 + j] + d2d[j]
     across_y = [
         go(remote(rs2.at[lax.rem(y + e, NY)], yrecv.at[e - 1], ys.at[e - 1], yr.at[e - 1], at_y(y + e)))
         for e in (2, 1, 3)
     ]
-    for copy in across_y:
-        copy.wait_recv()
+    arrive("ysum", *across_y)
     total = rs2[y]
     for e in range(NY - 1):
         total = total + yrecv[e]
@@ -338,12 +369,12 @@
         for e in range(1, NX)
     ]
     mixed[x] = ofin[0]
+    arrive("outs", *outs)
     for e in range(1, NX):
-        outs[e - 1].wait_recv()
         mixed[lax.rem(x + e, NX)] = orecv[e - 1]
-    out_s.wait()
-    for copy in pending:
-        copy.wait_send()
+    with jax.named_scope("drain"):
+        for copy in pending:
+            copy.wait_send()
 
 
 def fused(*operands):
@@ -351,6 +382,24 @@
     vmem = pl.BlockSpec(memory_space=pltpu.VMEM)
     dma = pltpu.SemaphoreType.DMA
     scratch = [
+        pltpu.VMEM((NX * NZ, 128), f32),
+        pltpu.VMEM((32, 512), bf16),
+        pltpu.VMEM((32, 512), bf16),
+        pltpu.VMEM((128, 128), bf16),
+        pltpu.VMEM((128, 128), bf16),
+        pltpu.VMEM((16, 8), f32),
+        pltpu.VMEM((16, 8), f32),
+        pltpu.VMEM((1, 8), jnp.int32),
+        pltpu.VMEM((1, 32), f32),
+        pltpu.VMEM((1, 128), f32),
+        dma((10,)),
+        pltpu.VMEM((128, 128), f32),
+        pltpu.VMEM((128, 128), f32),
+        pltpu.VMEM((NH, 64, 128), f32),
+        pltpu.VMEM((8, 2048), f32),
+        pltpu.VMEM((8, 2048), f32),
+        pltpu.VMEM((16, 512), bf16),
+        pltpu.VMEM((NX, 1, 128), f32),
         pltpu.VMEM((NX, NZ, 32, 128), bf16),
         pltpu.VMEM((4, NX, 128, 512), bf16),
         pltpu.VMEM((8, 256), f32),
@@ -365,7 +414,6 @@
         pltpu.VMEM((4, 3, 32, 512), bf16),
         pltpu.VMEM((4, 3, 32, 512), bf16),
         pltpu.VMEM((512, 512), bf16),
-        pltpu.VMEM((NB * NH, 128, 128), f32),
         pltpu.VMEM((NH, 64, 128), f32),
         pltpu.VMEM((NH, 64, 128), f32),
         pltpu.VMEM((NH, 64, 128), f32),
@@ -396,19 +444,15 @@
     return pl.pallas_call(
         kernel,
         out_shape=(
-            jax.ShapeDtypeStruct((NX, 32, 128), bf16),
-            jax.ShapeDtypeStruct((NB * NH, 128, 128), f32),
+            pltpu.VMEM((NX, 32, 128), bf16),
+            pltpu.VMEM((NB * NH, 128, 128), f32),
         ),
-        in_specs=[anywhere] * 7 + [vmem] * 8,
-        out_specs=(vmem, anywhere),
+        in_specs=[anywhere] * 17,
+        out_specs=(vmem, vmem),
         scratch_shapes=scratch,
         compiler_params=pltpu.CompilerParams(collective_id=0, has_side_effects=True),
         name="step",
     )(*operands)
-
-
-def unit_rows(values):
-    return values * lax.rsqrt(jnp.sum(values * values, axis=-1, keepdims=True) + epsilon)
 
 
 def per_device(
@@ -430,28 +474,12 @@
     prev_beta,
     accepted,
 ):
-    z = lax.axis_index("kv") // NX
-    head_start = lax.axis_index("tp") * NH
-    gain = lax.dynamic_slice_in_dim(norm_gain, z * 512, 512, 0).reshape(NX, 1, 128)
-    both = [lax.dynamic_slice(w, (z * 512, head_start), (512, NH)).T for w in (w_decay, w_beta)]
-    abw = jnp.concatenate(both + [jnp.zeros((8, 512), bf16)], axis=0)
-    abw = abw.reshape(16, NX, 128).transpose(1, 0, 2)
-    rate = jnp.pad(lax.dynamic_slice_in_dim(decay_rate, head_start, NH, 0), (0, 4))
-    rate = jnp.broadcast_to(rate[:, None], (8, 128))
-
-    def by_step(v):
-        return v.transpose(2, 0, 1, 3).reshape(NT, NB, NH * 128)
-
-    kold = unit_rows(prev_keys.astype(f32)).transpose(1, 0, 2, 3)
-    kold = jnp.pad(kold, ((0, 0), (0, 0), (0, 4), (0, 0))).reshape(NH, NB * 8, 128)
-    vold = by_step(prev_values.astype(f32))
-    keep = (jnp.arange(NT)[None, :] < accepted[:, None]).astype(f32)[:, None, :]
-    wide = (NB, NH, NT, 128)
-    gold = by_step(jnp.broadcast_to((prev_log_decay * keep)[..., None], wide))
-    bold = by_step(jnp.broadcast_to((prev_beta * keep)[..., None], wide))
     mixed, carried = fused(
         tokens.reshape(NZ, NX, 32, 128), w_key, w_query, w_value, w_gate, w_out,
-        state.reshape(NB * NH, 128, 128), gain, abw, kold, vold, gold, bold, rate, head_gain.reshape(1, 128),
+        state.reshape(NB * NH, 128, 128), norm_gain.reshape(NX * NZ, 128), w_decay.T, w_beta.T,
+        prev_keys.reshape(128, 128), prev_values.reshape(128, 128),
+        prev_log_decay.transpose(1, 2, 0).reshape(16, NB), prev_beta.transpose(1, 2, 0).reshape(16, NB),
+        accepted.reshape(1, NB), decay_rate.reshape(1, 32), head_gain.reshape(1, 128),
     )
     return mixed.reshape(32, NT, 128), carried.reshape(NB, NH, 128, 128)
 

time: 85.9 us -> 71.2 us (0.83)
  local copies, waits for them, and re-layouts: 9.55 us -> 1.94 us
  other arithmetic: 5.22 us -> 0 us
  Pallas kernels: 69.9 us -> 68.5 us
    unnamed x3 -> x2, local copies, waits for them, and re-layouts: 4.52 us -> 1.94 us
    reshape x2 -> x0, other arithmetic: 2.28 us -> none  [the longest x1 1.51 us: per_device(): jnp.pad(kold, ((0, 0), (0, 0), (0, 4), (0, 0))).reshape(NH, NB * 8, 128)]
    dynamic_slice x2 -> x0, local copies, waits for them, and re-layouts: 2.08 us -> none  [the longest x1 1.34 us: per_device(): lax.dynamic_slice_in_dim(norm_gain, z * 512, 512, 0).reshape(NX, 1, 128)]
    pallas_call x1, Pallas kernels: 69.9 us -> 68.5 us  [fused(): pl.pallas_call(kernel, out_shape=(pltpu.VMEM((NX, 32, 128), bf16), pltpu....]
    reshape x2 -> x0, local copies, waits for them, and re-layouts: 1.4 us -> none  [by_step(): return v.transpose(2, 0, 1, 3).reshape(NT, NB, NH * 128)]
    reduce_sum x1 -> x0, other arithmetic: 0.87 us -> none  [unit_rows(): jnp.sum(values * values, axis=-1, keepdims=True) + epsilon]
where the time goes in v2:
time: 71.2 us; the launch traced here: 71.1 us
  Pallas kernels  68.5 us (96%)
  local copies, waits for them, and re-layouts  1.94 us (3%)
    pallas_call x1, Pallas kernels, fused(): pl.pallas_call(kernel, out_shape=(pltpu.VMEM((NX, 32, 128), bf16), pltpu....  68.5 us
    unnamed x2, local copies, waits for them, and re-layouts  1.94 us

profile of v2, /device:TPU:1, one launch (start us, length us, event | category | flops | bytes accessed | tf_op | source)
XLA Modules:
  0.0 71.1 jit_solution(5262240882835484611)
XLA Ops:
  0.6 68.5 %step.1 = (bf16[4,32,128]{2,1,0:T(8,128)(2,1)S(1)}, f32[32,128,128]{2,1,0:T(8,128)S(1)}) custom-call(bf16[8,4,32,128]{3,2,1,0:T(8,128)(2,1)} %bitcast.21, bf16[128,512]{1,0:T(8,128)(2,1)} %wkey.1, bf16[128,512]{1,0:T(8,128)(2,1)} %wquery.1, bf16[128,512]{1,0:T(8,128)(2,1)} %wvalue.1, bf16[128,512]{1,0:T(8,128)(2,1)} %wgate.1, bf16[512,128]{1,0:T(8,128)(2,1)} %wout.1, ...), custom_call_target="tpu_custom_call" | custom-call | tf_op jit(solution)/shard_map/step/pallas_call | solution.py:444
  69.1 0.6 copy.21
  69.8 1.3 %copy.22 = f32[8,4,128,128]{3,2,1,0:T(8,128)} copy(f32[8,4,128,128]{3,2,1,0:T(8,128)S(1)} %bitcast.18) | data formatting | bytes 4194304

commit v3 on v2

--- a/solution.py
+++ b/solution.py
@@ -54,9 +54,9 @@
     small_ref, rest = rest[:10], rest[10:]
     gain, wdecay, wbeta, pkeys, pvalues, plogs, pbetas, accepted, rate, hgain = small_ref
     (
-    small_sem, kraw, vraw, kold, gold, bold, abw, gainrow, xtok, wbuf, stsend, strecv, scol, nbuf, absend, abrecv, yown, y1send, y1recv, y2send, y2recv,
-    wobuf, pbuf, ubuf, ebuf, tmp, kq, gnew, bnew, vnew, hout, hsend, hz, p3, d2d, rs2, yrecv, ofin, orecv,
-    loc, ts, tr, wds, wdr, wrs, wrr, sts, str_, abs_, abr, y1s, y1r, y2s, y2r, wos, wor, hs, hr, ds_, dr, ys, yr, os_, or_,
+    small_sem, kraw, vraw, kold, gold, bold, abw, gainrow, tokbuf, xtok, wbuf, stsend, strecv, scol, nbuf, absend, abrecv, yown, y1send, y1recv, y2send, y2recv,
+    wobuf, pbuf, ubuf, ebuf, tmp, kq, gnew, bnew, vnew, hout, hsend, hz, p3, d2d, psend, precv,
+    loc, ts, tr, wds, wdr, wrs, wrr, sts, str_, abs_, abr, y1s, y1r, y2s, y2r, wos, wor, hs, hr, tws, twr, ps, pr,
     ) = rest
     kv, tp = lax.axis_index("kv"), lax.axis_index("tp")
     z, x, y, c = kv // NX, lax.rem(kv, NX), tp // 2, lax.rem(tp, 2)
@@ -69,9 +69,6 @@
     def at_x(xx):
         return {"kv": z * NX + lax.rem(xx + NX, NX)}
 
-    def at_y(yy):
-        return {"tp": lax.rem(yy + NY, NY) * 2 + c}
-
     def dest(r):
         off = side * r if r < 4 else -side * (r - 3)
         return lax.rem(z + off + 2 * NZ, NZ)
@@ -94,54 +91,32 @@
             for copy in copies:
                 copy.wait_recv()
 
-    own_tok = pltpu.make_async_copy(tok.at[:, x], xtok.at[0], loc.at[0])
+    own_tok = pltpu.make_async_copy(tok, tokbuf, loc.at[0])
     own_tok.start()
     own_w = [pltpu.make_async_copy(weights[m], wbuf.at[m, 0], loc.at[1 + m]) for m in range(4)]
-    for copy in own_w:
-        copy.start()
-    own_s = pltpu.make_async_copy(state, sbuf, loc.at[5])
-    own_s.start()
+    own_w[0].start()
     sources = list(small_in)
     for i in (1, 2):
         sources[i] = small_in[i].at[:, pl.ds(pl.multiple_of(z * 512, 512), 512)]
     own_small = [pltpu.make_async_copy(a, b, small_sem.at[i]) for i, (a, b) in enumerate(zip(sources, small_ref))]
     for copy in own_small:
         copy.start()
+    own_s = pltpu.make_async_copy(state, sbuf, loc.at[5])
+    own_s.start()
+    for copy in own_w[1:]:
+        copy.start()
     own_wo = pltpu.make_async_copy(wout, wobuf.at[:, pl.ds(0, 128)], loc.at[6])
     own_wo.start()
 
     barrier = pltpu.get_barrier_semaphore()
-    for d in range(1, NX):
-        pl.semaphore_signal(barrier, inc=1, device_id=at_x(x + d), device_id_type=MESH)
+    for ey in range(NY):
+        for ex in range(NX):
+            if ey or ex:
+                there = {"kv": z * NX + lax.rem(x + ex, NX), "tp": lax.rem(y + ey, NY) * 2 + c}
+                pl.semaphore_signal(barrier, inc=1, device_id=there, device_id_type=MESH)
     for d in range(1, NZ):
         pl.semaphore_signal(barrier, inc=1, device_id=at_z(z + d), device_id_type=MESH)
-    for d in range(1, NY):
-        pl.semaphore_signal(barrier, inc=1, device_id=at_y(y + d), device_id_type=MESH)
     pl.semaphore_signal(barrier, inc=1, device_id=twin, device_id_type=MESH)
-    with jax.named_scope("barrier"):
-        pl.semaphore_wait(barrier, NX + NZ + NY - 2)
-
-    toks = [
-        go(remote(tok.at[:, lax.rem(x + d, NX)], xtok.at[d], ts.at[d - 1], tr.at[d - 1], at_x(x + d)))
-        for d in range(1, NX)
-    ]
-
-    def direct(m):
-        return [
-            go(remote(weights[m], wbuf.at[m, 1], wds.at[m, 0], wdr.at[m, 0], at_x(x + 1))),
-            go(remote(weights[m], wbuf.at[m, 3], wds.at[m, 1], wdr.at[m, 1], at_x(x + 3))),
-        ]
-
-    def relay(m, copies):
-        low, high = pl.ds(0, 64), pl.ds(64, 64)
-        arrive(f"left{m}", copies[0])
-        first = go(remote(wbuf.at[m, 1, low], wbuf.at[m, 2, low], wrs.at[m, 0], wrr.at[m, 0], at_x(x + 1)))
-        arrive(f"right{m}", copies[1])
-        second = go(remote(wbuf.at[m, 3, high], wbuf.at[m, 2, high], wrs.at[m, 1], wrr.at[m, 1], at_x(x + 3)))
-        return [first, second]
-
-    d0 = direct(0)
-    d1 = direct(1)
 
     for copy in own_small:
         copy.wait()
@@ -167,35 +142,94 @@
     spread = spread.astype(f32)
     gold[...] = contract(jnp.where(kept, plogs[...], 0.0), spread, ((0,), (0,)), HIGHEST)
     bold[...] = contract(jnp.where(kept, pbetas[...], 0.0), spread, ((0,), (0,)), HIGHEST)
-
     own_tok.wait()
-    arrive("tokens", *toks)
+    own_w[0].wait()
+    with jax.named_scope("barrier"):
+        pl.semaphore_wait(barrier, NX * NY + NZ - 1)
+
+    mine = pl.ds(c * 4, 4)
+    toks = [
+        go(remote(tokbuf.at[mine, lax.rem(x + d, NX)], xtok.at[d, mine], ts.at[d - 1], tr.at[d - 1], at_x(x + d)))
+        for d in range(1, NX)
+    ]
+
+    def direct(m):
+        return [
+            go(remote(wbuf.at[m, 0], wbuf.at[m, 1], wds.at[m, 0], wdr.at[m, 0], at_x(x + 1))),
+            go(remote(wbuf.at[m, 0], wbuf.at[m, 3], wds.at[m, 1], wdr.at[m, 1], at_x(x + 3))),
+        ]
+
+    def relay(m, copies):
+        low, high = pl.ds(0, 64), pl.ds(64, 64)
+        arrive(f"left{m}", copies[0])
+        first = go(remote(wbuf.at[m, 1, low], wbuf.at[m, 2, low], wrs.at[m, 0], wrr.at[m, 0], at_x(x + 1)))
+        arrive(f"right{m}", copies[1])
+        second = go(remote(wbuf.at[m, 3, high], wbuf.at[m, 2, high], wrs.at[m, 1], wrr.at[m, 1], at_x(x + 3)))
+        return [first, second]
+
+    d0 = direct(0)
+    own_w[1].wait()
+    d1 = direct(1)
+
+    def products(left, b, h):
+        rows = pl.ds(pl.multiple_of(b * 8, 8), 8)
+        pbuf[h, rows] = contract(left[h, rows], sbuf[b * NH + h], ((1,), (0,)), HIGHEST)
+
+    def all_products(left, first, last):
+        @pl.loop(first, last)
+        def _(b):
+            for h in range(NH):
+                products(left, b, h)
+
+    def every(ref, start, h):
+        return ref[h, pl.ds(start, 8, stride=8)]
+
+    def update_state(first, last):
+        @pl.loop(first, last)
+        def _(b):
+            rows = pl.ds(pl.multiple_of(b * 8, 8), 8)
+            for h in range(NH):
+                added = contract(kold[h, rows], ubuf[h, rows], ((0,), (0,)), HIGHEST)
+                sbuf[b * NH + h] = sbuf[b * NH + h] * ebuf[h, rows][0:1] + added
+
+    own_s.wait()
+    all_products(kold, 0, NB)
+
+    shared = []
+    for d in (1, 3, 2):
+        arrive(f"tokens{d}", toks[d - 1])
+        shared.append(
+            go(remote(xtok.at[d, mine], xtok.at[d, mine], tws.at[d - 1], twr.at[d - 1], twin))
+        )
+    xtok[0] = tokbuf[:, x]
+    arrive("tokens", *shared)
     squares = jnp.zeros((NZ * 32, 128), f32)
     for d in range(NX):
         part = xtok[d].reshape(NZ * 32, 128).astype(f32)
         squares = squares + part * part
     stsend[...] = contract(jnp.ones((8, 128), f32), squares, ((1,), (1,)), HIGHEST)
     stats = [
-        go(remote(stsend, strecv.at[d - 1], sts.at[d - 1], str_.at[d - 1], at_z(z + d))) for d in range(1, NZ)
+        go(remote(stsend, strecv.at[d - 1], sts.at[d - 1], str_.at[d - 1], at_z(z + d))) for d in (4, 3, 5, 2, 6, 1, 7)
     ]
 
-    def products(left, b, h):
-        rows = pl.ds(pl.multiple_of(b * 8, 8), 8)
-        pbuf[h, rows] = contract(left[h, rows], sbuf[b * NH + h], ((1,), (0,)), HIGHEST)
-
-    def all_products(left):
-        @pl.loop(0, NB)
-        def _(b):
-            for h in range(NH):
-                products(left, b, h)
-
-    def every(ref, start, h):
-        return ref[h, pl.ds(start, 8, stride=8)]
-
-    own_s.wait()
-    all_products(kold)
+    for h in range(NH):
+        keys = [every(kold, t, h) for t in range(NT)]
+        written, decay = delta_rule(
+            keys,
+            [every(pbuf, t, h) for t in range(NT)],
+            [vraw[pl.ds(h * NT + t, 8, stride=16)] for t in range(NT)],
+            [gold[:, head(h * NT + t)] for t in range(NT)],
+            [bold[:, head(h * NT + t)] for t in range(NT)],
+        )
+        for t in range(NT):
+            last = written[t] if t == NT - 1 else decay[NT - 1, t] * written[t]
+            ubuf[h, pl.ds(t, 8, stride=8)] = last
+            ubuf[h, pl.ds(t + 4, 8, stride=8)] = jnp.zeros((8, 128), f32)
+        ebuf[h, pl.ds(0, 8, stride=8)] = decay[NT - 1, -1]
+    update_state(0, 4)
 
     r0 = relay(0, d0)
+    own_w[2].wait()
     d2 = direct(2)
 
     arrive("stats", *stats)
@@ -205,6 +239,9 @@
     scale = lax.rsqrt(total * (1.0 / (NX * NZ * 128)) + epsilon)
     first_row = (lax.broadcasted_iota(jnp.int32, (8, 128), 0) == 0).astype(f32)
     scol[...] = contract(scale, first_row, ((0,), (0,)), HIGHEST).reshape(NZ, 32, 128)
+    r1 = relay(1, d1)
+    own_w[3].wait()
+    d3 = direct(3)
     absend[...] = jnp.zeros((NZ, 8, 128), f32)
     for r in range(NZ):
         zz = dest(r)
@@ -221,20 +258,28 @@
     ]
 
     def project(m, copies):
-        own_w[m].wait()
         arrive(f"far{m}", *copies)
         rows = jnp.dot(nbuf[...], wbuf[m].reshape(512, 512), preferred_element_type=f32)
-        yown[m] = rows[0:128]
-        y1send[m] = rows[128:256].astype(bf16)
-        return go(remote(y1send.at[m], y1recv.at[m], y1s.at[m], y1r.at[m], at_z(z + (-side))))
+        if m % 2 == 0:
+            yown[m] = rows[0:128]
+            y1send[m] = rows[128:256].astype(bf16)
+            other = z - side
+        else:
+            yown[m, 0:32] = rows[0:32]
+            yown[m, 32:128] = rows[128:224]
+            y1send[m, 0:96] = rows[32:128].astype(bf16)
+            y1send[m, 96:128] = rows[224:256].astype(bf16)
+            other = z + side
+        return go(remote(y1send.at[m], y1recv.at[m], y1s.at[m], y1r.at[m], at_z(other)))
 
     def second_sum(m, copy):
         arrive(f"pair{m}", copy)
         rows = yown[m] + y1recv[m].astype(f32)
         yown[m, 0:32] = rows[0:32]
         y2send[m] = rows[32:128].astype(bf16).reshape(3, 32, 512)
+        way = side if m % 2 == 0 else -side
         return [
-            go(remote(y2send.at[m, i - 1], y2recv.at[m, i - 1], y2s.at[m, i - 1], y2r.at[m, i - 1], at_z(dest(i))))
+            go(remote(y2send.at[m, i - 1], y2recv.at[m, i - 1], y2s.at[m, i - 1], y2r.at[m, i - 1], at_z(z + way * i)))
             for i in (3, 2, 1)
         ]
 
@@ -245,42 +290,17 @@
         return rows
 
     y1_0 = project(0, r0)
-    r1 = relay(1, d1)
-    d3 = direct(3)
-
-    for h in range(NH):
-        keys = [every(kold, t, h) for t in range(NT)]
-        written, decay = delta_rule(
-            keys,
-            [every(pbuf, t, h) for t in range(NT)],
-            [vraw[pl.ds(h * NT + t, 8, stride=16)] for t in range(NT)],
-            [gold[:, head(h * NT + t)] for t in range(NT)],
-            [bold[:, head(h * NT + t)] for t in range(NT)],
-        )
-        for t in range(NT):
-            last = written[t] if t == NT - 1 else decay[NT - 1, t] * written[t]
-            ubuf[h, pl.ds(t, 8, stride=8)] = last
-            ubuf[h, pl.ds(t + 4, 8, stride=8)] = jnp.zeros((8, 128), f32)
-        ebuf[h, pl.ds(0, 8, stride=8)] = decay[NT - 1, -1]
-
+    r2 = relay(2, d2)
+    y1_1 = project(1, r1)
     y2_0 = second_sum(0, y1_0)
-    y1_1 = project(1, r1)
-    r2 = relay(2, d2)
+    r3 = relay(3, d3)
     wos_ = [
         go(remote(wout, wobuf.at[:, pl.ds(d * 128, 128)], wos.at[d - 1], wor.at[d - 1], at_x(x + d)))
         for d in range(1, NX)
     ]
-
-    @pl.loop(0, NB)
-    def _(b):
-        rows = pl.ds(pl.multiple_of(b * 8, 8), 8)
-        for h in range(NH):
-            added = contract(kold[h, rows], ubuf[h, rows], ((0,), (0,)), HIGHEST)
-            sbuf[b * NH + h] = sbuf[b * NH + h] * ebuf[h, rows][0:1] + added
-
+    update_state(4, NB)
+    y1_2 = project(2, r2)
     y2_1 = second_sum(1, y1_1)
-    y1_2 = project(2, r2)
-    r3 = relay(3, d3)
 
     arrive("small", *ab)
     small = absend[0]
@@ -289,8 +309,8 @@
     soft = jnp.maximum(small, 0.0) + jnp.log1p(jnp.exp(-jnp.abs(small)))
     which = lax.broadcasted_iota(jnp.int32, (8, 128), 0)
     lane = lax.broadcasted_iota(jnp.int32, (8, 32), 1)
-    mine = lane == tp * NH + lax.broadcasted_iota(jnp.int32, (8, 32), 0)
-    rates = jnp.sum(jnp.where(mine, rate[...], 0.0), axis=1, keepdims=True)
+    chosen = lane == tp * NH + lax.broadcasted_iota(jnp.int32, (8, 32), 0)
+    rates = jnp.sum(jnp.where(chosen, rate[...], 0.0), axis=1, keepdims=True)
     small = jnp.where(which < NH, -rates * soft, 1.0 / (1.0 + jnp.exp(-small)))
     row = lax.broadcasted_iota(jnp.int32, (8, 512), 0)
     lane = lax.broadcasted_iota(jnp.int32, (8, 512), 1) // 128
@@ -301,21 +321,24 @@
         bnew[h] = strengths[0:32, head(h)]
 
     y1_3 = project(3, r3)
-    y2_2 = second_sum(2, y1_2)
 
     def rows_of(ref, t, h):
         return ref[h, pl.ds(t, 8, stride=4)]
 
-    for m, copies, factor in ((0, y2_0, 1.0), (1, y2_1, 128**-0.5)):
+    def unit_rows(m, copies, factor):
         arrive(f"sum{m}", *copies)
         for h in range(NH):
             v = silu(summed(m, copies, head(h)))
             tmp[h] = v * lax.rsqrt(across(v * v) + epsilon) * factor
             for t in range(NT):
                 kq[h, pl.ds(m * 4 + t, 8, stride=8)] = rows_of(tmp, t, h)
-    all_products(kq)
-
+
+    unit_rows(0, y2_0, 1.0)
+    y2_2 = second_sum(2, y1_2)
+    unit_rows(1, y2_1, 128**-0.5)
+    all_products(kq, 0, 4)
     y2_3 = second_sum(3, y1_3)
+    all_products(kq, 4, NB)
     arrive("sum2", *y2_2)
     for h in range(NH):
         vnew[h] = silu(summed(2, y2_2, head(h)))
@@ -348,30 +371,29 @@
     terms = jnp.dot(hz[...].reshape(256, 512), wobuf[...], preferred_element_type=f32)
     for d in range(NZ):
         zz = lax.rem(z + NZ - d, NZ)
-        p3[lax.rem(zz, 2) * 4 + zz // 2] = terms[d * 32 : (d + 1) * 32]
-    other = go(remote(p3.at[pl.ds((1 - c) * 4, 4)], d2d, ds_, dr, twin))
+        p3[lax.rem(zz, 2) * NY + zz // 2] = terms[d * 32 : (d + 1) * 32]
+    other = go(remote(p3.at[pl.ds((1 - c) * NY, NY)], d2d, tws.at[3], twr.at[3], twin))
     arrive("twin", other)
     for j in range(NY):
-        rs2[j] = p3[c * 4 + j] + d2d[j]
-    across_y = [
-        go(remote(rs2.at[lax.rem(y + e, NY)], yrecv.at[e - 1], ys.at[e - 1], yr.at[e - 1], at_y(y + e)))
-        for e in (2, 1, 3)
+        rows = p3[c * NY + j] + d2d[j]
+        for e in range(NX):
+            psend[j, e] = rows[:, head(e)].astype(bf16)
+    parts = [
+        go(
+            remote(
+                psend.at[lax.rem(y + ey, NY), ex], precv.at[ey, ex], ps.at[ey, ex], pr.at[ey, ex],
+                {"kv": z * NX + lax.rem(x + NX - ex, NX), "tp": lax.rem(y + ey, NY) * 2 + c},
+            )
+        )
+        for ey, ex in ((2, 2), (2, 1), (2, 3), (1, 2), (3, 2), (2, 0), (0, 2), (1, 1), (1, 3), (3, 1), (3, 3), (1, 0), (3, 0), (0, 1), (0, 3))
     ]
-    arrive("ysum", *across_y)
-    total = rs2[y]
-    for e in range(NY - 1):
-        total = total + yrecv[e]
-    total = total.astype(bf16)
-    for e in range(NX):
-        ofin[e] = total[:, head(e)]
-    outs = [
-        go(remote(ofin.at[e], orecv.at[e - 1], os_.at[e - 1], or_.at[e - 1], at_x(x + NX - e)))
-        for e in range(1, NX)
-    ]
-    mixed[x] = ofin[0]
-    arrive("outs", *outs)
-    for e in range(1, NX):
-        mixed[lax.rem(x + e, NX)] = orecv[e - 1]
+    own_part = p3[c * NY + y, :, 0:128] + d2d[y, :, 0:128]
+    arrive("parts", *parts)
+    for ex in range(NX):
+        total = own_part if ex == 0 else precv[0, ex].astype(f32)
+        for ey in range(1, NY):
+            total = total + precv[ey, ex].astype(f32)
+        mixed[lax.rem(x + ex, NX)] = total.astype(bf16)
     with jax.named_scope("drain"):
         for copy in pending:
             copy.wait_send()
@@ -400,6 +422,7 @@
         pltpu.VMEM((8, 2048), f32),
         pltpu.VMEM((16, 512), bf16),
         pltpu.VMEM((NX, 1, 128), f32),
+        pltpu.VMEM((NZ, NX, 32, 128), bf16),
         pltpu.VMEM((NX, NZ, 32, 128), bf16),
         pltpu.VMEM((4, NX, 128, 512), bf16),
         pltpu.VMEM((8, 256), f32),
@@ -427,10 +450,8 @@
         pltpu.VMEM((NZ, 32, 512), bf16),
         pltpu.VMEM((NZ, 32, 512), f32),
         pltpu.VMEM((NY, 32, 512), f32),
-        pltpu.VMEM((NY, 32, 512), f32),
-        pltpu.VMEM((NY - 1, 32, 512), f32),
-        pltpu.VMEM((NX, 32, 128), bf16),
-        pltpu.VMEM((NX - 1, 32, 128), bf16),
+        pltpu.VMEM((NY, NX, 32, 128), bf16),
+        pltpu.VMEM((NY, NX, 32, 128), bf16),
         dma((8,)),
         dma((3,)), dma((3,)),
         dma((4, 2)), dma((4, 2)), dma((4, 2)), dma((4, 2)),
@@ -438,8 +459,8 @@
         dma((4,)), dma((4,)), dma((4, 3)), dma((4, 3)),
         dma((3,)), dma((3,)),
         dma((7,)), dma((7,)),
-        dma, dma,
-        dma((3,)), dma((3,)), dma((3,)), dma((3,)),
+        dma((4,)), dma((4,)),
+        dma((NY, NX)), dma((NY, NX)),
     ]
     return pl.pallas_call(
         kernel,

time: 71.2 us -> 64.1 us (0.900)
  Pallas kernels: 68.5 us -> 61.3 us
    pallas_call x1, Pallas kernels: 68.5 us -> 61.3 us  [fused(): pl.pallas_call(kernel, out_shape=(pltpu.VMEM((NX, 32, 128), bf16), pltpu....]
where the time goes in v3:
time: 64.1 us; the launch traced here: 63.9 us
  Pallas kernels  61.3 us (96%)
  local copies, waits for them, and re-layouts  1.94 us (3%)
  between operations  0.65 us (1%)
    pallas_call x1, Pallas kernels, fused(): pl.pallas_call(kernel, out_shape=(pltpu.VMEM((NX, 32, 128), bf16), pltpu....  61.3 us
    unnamed x2, local copies, waits for them, and re-layouts  1.94 us

profile of v3, /device:TPU:1, one launch (start us, length us, event | category | flops | bytes accessed | tf_op | source)
XLA Modules:
  0.0 63.9 jit_solution(2775761653452598583)
XLA Ops:
  0.6 61.3 %step.1 = (bf16[4,32,128]{2,1,0:T(8,128)(2,1)S(1)}, f32[32,128,128]{2,1,0:T(8,128)S(1)}) custom-call(bf16[8,4,32,128]{3,2,1,0:T(8,128)(2,1)} %bitcast.21, bf16[128,512]{1,0:T(8,128)(2,1)} %wkey.1, bf16[128,512]{1,0:T(8,128)(2,1)} %wquery.1, bf16[128,512]{1,0:T(8,128)(2,1)} %wvalue.1, bf16[128,512]{1,0:T(8,128)(2,1)} %wgate.1, bf16[512,128]{1,0:T(8,128)(2,1)} %wout.1, ...), custom_call_target="tpu_custom_call" | custom-call | tf_op jit(solution)/shard_map/step/pallas_call | solution.py:465
  62.0 0.6 copy.21
  62.6 1.3 %copy.22 = f32[8,4,128,128]{3,2,1,0:T(8,128)} copy(f32[8,4,128,128]{3,2,1,0:T(8,128)S(1)} %bitcast.18) | data formatting | bytes 4194304

commit v4 on v3

v4 whole, which is shorter than its diff:
```python
import jax
import jax.numpy as jnp
from jax import lax
from jax.experimental import pallas as pl
from jax.experimental.pallas import tpu as pltpu
from jax.sharding import PartitionSpec as P

MESH = pl.DeviceIdType.MESH
HIGHEST = lax.Precision.HIGHEST
epsilon = 1e-06

NZ, NX, NY, NT, NB, NH = 8, 4, 4, 4, 8, 4
f32, bf16 = jnp.float32, jnp.bfloat16
NC, WIDE = 8, 256
CHUNKS = tuple(slice(i * WIDE, (i + 1) * WIDE) for i in range(NC))


def contract(a, b, dims, precision=None):
    return lax.dot_general(a, b, (dims, ((), ())), precision=precision, preferred_element_type=f32)


def silu(v):
    return v / (1.0 + jnp.exp(-v))


def head(h):
    return slice(h * 128, (h + 1) * 128)


def across(v):
    return jnp.sum(v, axis=-1, keepdims=True)


def delta_rule(keys, predicted, values, logs, betas):
    decay = {}
    for t in range(NT):
        total = logs[t]
        decay[t, t] = None
        for i in range(t - 1, -1, -1):
            decay[t, i] = jnp.exp(total)
            total = total + logs[i]
        decay[t, -1] = jnp.exp(total)
    written = []
    for t in range(NT):
        expected = decay[t, -1] * predicted[t]
        for i in range(t):
            expected = expected + decay[t, i] * across(keys[i] * keys[t]) * written[i]
        written.append(betas[t] * (values[t] - expected))
    return written, decay


def kernel(
    tok, wkey, wquery, wvalue, wgate, wout, state, *rest
):
    small_in, (mixed, sbuf, *rest) = rest[:10], rest[10:]
    small_ref, rest = rest[:10], rest[10:]
    gain, wdecay, wbeta, pkeys, pvalues, plogs, pbetas, accepted, rate, hgain = small_ref
    (
    small_sem, kraw, vraw, kold, gold, bold, abw, gainrow, tokbuf, xtok, wbuf, sqsend, sqrecv, stsend, strecv, scol, nbuf, absend, abrecv,
    yown, y1send, y1recv, y2send, y2recv, wobuf, halves, pbuf, ubuf, ebuf, tmp, kq, gnew, bnew, vnew, hout,
    hsend, hz, p3, d2d, psend, precv,
    loc, tr, wdr, wrr, y1r, y2r, hr, hs, sent, got, wave,
    ) = rest
    s_sq, s_tok, s_direct, s_relay, s_stat, s_small, s_y1, s_y2, s_wo, s_twin, s_d2d, s_part = [sent.at[i] for i in range(12)]
    r_sq, r_stat, r_small, r_wo, r_twin, r_d2d, r_part = [got.at[i] for i in range(7)]
    kv, tp = lax.axis_index("kv"), lax.axis_index("tp")
    z, x, y, c = kv // NX, lax.rem(kv, NX), tp // 2, lax.rem(tp, 2)
    side = 2 * lax.rem(z, 2) - 1
    weights = (wkey, wquery, wvalue, wgate)

    def at_z(zz):
        return {"kv": lax.rem(zz + 2 * NZ, NZ) * NX + x}

    def at_x(xx):
        return {"kv": z * NX + lax.rem(xx + NX, NX)}

    def dest(r):
        off = side * r if r < 4 else -side * (r - 3)
        return lax.rem(z + off + 2 * NZ, NZ)

    def remote(src, dst, send, recv, device):
        return pltpu.make_async_remote_copy(
            src_ref=src, dst_ref=dst, send_sem=send, recv_sem=recv, device_id=device, device_id_type=MESH
        )

    twin = {"tp": tp + 1 - 2 * c}

    def go(copy):
        copy.start()
        return copy

    def arrive(name, ref, sem):
        with jax.named_scope(name):
            pltpu.make_async_copy(ref, ref, sem).wait()

    barrier = pltpu.get_barrier_semaphore()
    near = [at_x(x + d) for d in (1, 3, 2)] + [at_z(z + 1), at_z(z - 1)]
    near += [{"tp": lax.rem(y + d, NY) * 2 + c} for d in (1, 3, 2)]
    for there in near:
        pl.semaphore_signal(barrier, inc=1, device_id=there, device_id_type=MESH)
    pl.semaphore_signal(barrier, inc=1, device_id=twin, device_id_type=MESH)

    own_tok = pltpu.make_async_copy(tok, tokbuf, loc.at[0])
    own_tok.start()
    own_w = []
    for i, lanes in enumerate(CHUNKS):
        m, start = lanes.start // 512, lanes.start % 512
        part = weights[m].at[:, pl.ds(start, lanes.stop - lanes.start)]
        own_w.append(pltpu.make_async_copy(part, wbuf.at[0, :, lanes], loc.at[3 + i]))
    for copy in own_w:
        copy.start()
    sources = list(small_in)
    for i in (1, 2):
        sources[i] = small_in[i].at[:, pl.ds(pl.multiple_of(z * 512, 512), 512)]
    own_small = [pltpu.make_async_copy(a, b, small_sem.at[i]) for i, (a, b) in enumerate(zip(sources, small_ref))]
    for copy in own_small:
        copy.start()
    own_s = pltpu.make_async_copy(state, sbuf, loc.at[1])
    own_s.start()
    own_wo = pltpu.make_async_copy(wout, wobuf.at[:, 0:128], loc.at[2])
    own_wo.start()

    own_tok.wait()
    for e in range(NX):
        squares = tokbuf[:, e].reshape(NZ * 32, 128).astype(f32)
        sqsend[e] = contract(jnp.ones((8, 128), f32), squares * squares, ((1,), (1,)), HIGHEST)[0:1]
    for copy in own_w:
        copy.wait()
    with jax.named_scope("barrier"):
        pl.semaphore_wait(barrier, len(near) + 1)

    for d in (2, 1, 3):
        go(remote(sqsend.at[lax.rem(x + d, NX)], sqrecv.at[d - 1], s_sq, r_sq, at_x(x + d)))

    mine, theirs = pl.ds(c * 4, 4), pl.ds(4 - c * 4, 4)
    for d in (2, 1, 3):
        go(remote(tokbuf.at[mine, lax.rem(x + d, NX)], xtok.at[d, mine], s_tok, tr.at[d - 1], at_x(x + d)))

    low, high = slice(0, 64), slice(64, 128)

    def direct(i):
        lanes = CHUNKS[i]
        go(remote(wbuf.at[0, :, lanes], wbuf.at[1, :, lanes], s_direct, wdr.at[i, 0], at_x(x + 1)))
        go(remote(wbuf.at[0, :, lanes], wbuf.at[3, :, lanes], s_direct, wdr.at[i, 1], at_x(x + 3)))

    def relay(i):
        lanes = CHUNKS[i]
        arrive(f"left{i}", wbuf.at[1, :, lanes], wdr.at[i, 0])
        go(remote(wbuf.at[1, low, lanes], wbuf.at[2, low, lanes], s_relay, wrr.at[i], at_x(x + 1)))
        arrive(f"right{i}", wbuf.at[3, :, lanes], wdr.at[i, 1])
        go(remote(wbuf.at[3, high, lanes], wbuf.at[2, high, lanes], s_relay, wrr.at[i], at_x(x + 3)))

    direct(0)
    direct(1)
    direct(2)

    def products(left, b, h):
        rows = pl.ds(pl.multiple_of(b * 8, 8), 8)
        pbuf[h, rows] = contract(left[h, rows], sbuf[b * NH + h], ((1,), (0,)), HIGHEST)

    def all_products(left, first, last):
        @pl.loop(first, last)
        def _(b):
            for h in range(NH):
                products(left, b, h)

    def every(ref, start, h):
        return ref[h, pl.ds(start, 8, stride=8)]

    def update_state(first, last):
        @pl.loop(first, last)
        def _(b):
            rows = pl.ds(pl.multiple_of(b * 8, 8), 8)
            for h in range(NH):
                added = contract(kold[h, rows], ubuf[h, rows], ((0,), (0,)), HIGHEST)
                matrix = sbuf[b * NH + h] * ebuf[h, rows][0:1] + added
                sbuf[b * NH + h] = matrix
                large = matrix.astype(bf16)
                halves[b * NH + h, 0:128] = large
                halves[b * NH + h, 128:256] = (matrix - large.astype(f32)).astype(bf16)

    def spread(k):
        pl.semaphore_signal(wave.at[k], inc=1, device_id=at_z(z + 1), device_id_type=MESH)
        pl.semaphore_signal(wave.at[k], inc=1, device_id=at_z(z - 1), device_id_type=MESH)

    spread(0)

    for copy in own_small:
        copy.wait()
    row = lax.broadcasted_iota(jnp.int32, (16, 32), 0)
    col = lax.broadcasted_iota(jnp.int32, (16, 32), 1) - tp * NH
    abw[...] = (
        contract(((row == col) & (row < NH)).astype(bf16), wdecay[...], ((1,), (0,)))
        + contract(((row == col + NH) & (row >= NH) & (row < 2 * NH)).astype(bf16), wbeta[...], ((1,), (0,)))
    ).astype(bf16)
    row = lax.broadcasted_iota(jnp.int32, (NX * NZ, 128), 0)
    for d in range(NX):
        here = row == z * NX + lax.rem(x + NX - d, NX)
        gainrow[d] = jnp.sum(jnp.where(here, gain[...], 0.0), axis=0, keepdims=True)
    pl.semaphore_wait(wave.at[0], 2)
    spread(1)
    keys = pkeys[...].astype(f32)
    kraw[...] = keys * lax.rsqrt(across(keys * keys) + epsilon)
    vraw[...] = pvalues[...].astype(f32)
    for h in range(NH):
        for t in range(NT):
            kold[h, pl.ds(t, 8, stride=8)] = kraw[pl.ds(h * NT + t, 8, stride=16)]
            kold[h, pl.ds(t + 4, 8, stride=8)] = jnp.zeros((8, 128), f32)
    kept = lax.rem(lax.broadcasted_iota(jnp.int32, (16, 8), 0), NT) < accepted[...]
    apart = lax.broadcasted_iota(jnp.int32, (16, 2048), 0) == lax.broadcasted_iota(jnp.int32, (16, 2048), 1) // 128
    apart = apart.astype(f32)
    gold[...] = contract(jnp.where(kept, plogs[...], 0.0), apart, ((0,), (0,)), HIGHEST)
    bold[...] = contract(jnp.where(kept, pbetas[...], 0.0), apart, ((0,), (0,)), HIGHEST)
    pl.semaphore_wait(wave.at[1], 2)
    spread(2)
    own_s.wait()
    all_products(kold, 0, 2)
    arrive("squares", sqrecv, r_sq)
    with jax.named_scope("wave"):
        pl.semaphore_wait(wave.at[2], 2)
    stsend[...] = ((sqsend[x] + sqrecv[0]) + sqrecv[1]) + sqrecv[2]
    for d in (4, 3, 5, 2, 6, 1, 7):
        go(remote(stsend, strecv.at[d - 1], s_stat, r_stat, at_z(z + d)))
    for d in (1, 3, 2):
        arrive(f"tokens{d}", xtok.at[d, mine], tr.at[d - 1])
        go(remote(xtok.at[d, mine], xtok.at[d, mine], s_twin, r_twin, twin))
    xtok[0] = tokbuf[:, x]
    relay(0)
    direct(3)
    all_products(kold, 2, NB)
    relay(1)
    direct(4)
    arrive("tokens", xtok.at[1:4, theirs], r_twin)

    for h in range(NH):
        keys = [every(kold, t, h) for t in range(NT)]
        written, decay = delta_rule(
            keys,
            [every(pbuf, t, h) for t in range(NT)],
            [vraw[pl.ds(h * NT + t, 8, stride=16)] for t in range(NT)],
            [gold[:, head(h * NT + t)] for t in range(NT)],
            [bold[:, head(h * NT + t)] for t in range(NT)],
        )
        for t in range(NT):
            last = written[t] if t == NT - 1 else decay[NT - 1, t] * written[t]
            ubuf[h, pl.ds(t, 8, stride=8)] = last
            ubuf[h, pl.ds(t + 4, 8, stride=8)] = jnp.zeros((8, 128), f32)
        ebuf[h, pl.ds(0, 8, stride=8)] = decay[NT - 1, -1]
    relay(2)
    direct(5)

    arrive("stats", strecv, r_stat)
    total = stsend[...]
    for d in range(NZ - 1):
        total = total + strecv[d]
    scale = lax.rsqrt(total * (1.0 / (NX * NZ * 128)) + epsilon)
    first_row = (lax.broadcasted_iota(jnp.int32, (8, 128), 0) == 0).astype(f32)
    scol[...] = contract(jnp.broadcast_to(scale, (8, 256)), first_row, ((0,), (0,)), HIGHEST).reshape(NZ, 32, 128)
    absend[...] = jnp.zeros((NZ, 8, 128), f32)
    for r in range(NZ):
        zz = dest(r)
        small = jnp.zeros((16, 32), f32)
        for d in range(NX):
            feature = lax.rem(x + NX - d, NX)
            normed = (xtok[d, zz].astype(f32) * scol[zz] * gainrow[d]).astype(bf16)
            nbuf[r * 32 : (r + 1) * 32, head(d)] = normed
            small = small + contract(abw[:, pl.ds(pl.multiple_of(feature * 128, 128), 128)], normed, ((1,), (1,)))
        absend[r, :, 0:32] = small[0:8]
    for r in range(1, NZ):
        go(remote(absend.at[r], abrecv.at[r - 1], s_small, r_small, at_z(dest(r))))
    def project(i):
        lanes = CHUNKS[i]
        arrive(f"far{i}", wbuf.at[2, :, lanes], wrr.at[i])
        rows = jnp.dot(
            nbuf[...], wbuf[:, :, lanes].reshape(512, lanes.stop - lanes.start), preferred_element_type=f32
        )
        if i % 2 == 0:
            yown[:, lanes] = rows[0:128]
            y1send[:, lanes] = rows[128:256].astype(bf16)
            other = z - side
        else:
            yown[0:32, lanes] = rows[0:32]
            yown[32:128, lanes] = rows[128:224]
            y1send[0:96, lanes] = rows[32:128].astype(bf16)
            y1send[96:128, lanes] = rows[224:256].astype(bf16)
            other = z + side
        go(remote(y1send.at[:, lanes], y1recv.at[:, lanes], s_y1, y1r.at[i], at_z(other)))

    def second_sum(i):
        lanes = CHUNKS[i]
        arrive(f"pair{i}", y1recv.at[:, lanes], y1r.at[i])
        rows = yown[:, lanes] + y1recv[:, lanes].astype(f32)
        yown[0:32, lanes] = rows[0:32]
        for j in range(3):
            y2send[j, :, lanes] = rows[32 * (j + 1) : 32 * (j + 2)].astype(bf16)
        way = side if i % 2 == 0 else -side
        for j in (3, 2, 1):
            go(remote(y2send.at[j - 1, :, lanes], y2recv.at[j - 1, :, lanes], s_y2, y2r.at[i], at_z(z + way * j)))

    def last_sum(i):
        lanes = CHUNKS[i]
        arrive(f"sum{i}", y2recv.at[:, :, lanes], y2r.at[i])

    def summed(m, h):
        lanes = head(m * NH + h)
        rows = yown[0:32, lanes]
        for j in range(3):
            rows = rows + y2recv[j, :, lanes].astype(f32)
        return rows

    project(0)
    relay(3)
    direct(6)
    project(1)
    update_state(0, 2)
    relay(4)
    direct(7)
    project(2)
    relay(5)
    update_state(2, 3)
    project(3)
    second_sum(0)
    relay(6)
    update_state(3, 4)
    second_sum(1)
    project(4)
    relay(7)
    own_wo.wait()
    for d in range(1, NX):
        go(remote(wobuf.at[:, 0:128], wobuf.at[:, d * 128 : (d + 1) * 128], s_wo, r_wo, at_x(x + d)))
    update_state(4, 5)
    second_sum(2)
    project(5)
    project(6)
    second_sum(3)
    project(7)
    update_state(5, NB)
    second_sum(4)

    arrive("small", abrecv, r_small)
    small = absend[0]
    for r in range(NZ - 1):
        small = small + abrecv[r]
    soft = jnp.maximum(small, 0.0) + jnp.log1p(jnp.exp(-jnp.abs(small)))
    which = lax.broadcasted_iota(jnp.int32, (8, 128), 0)
    lane = lax.broadcasted_iota(jnp.int32, (8, 32), 1)
    chosen = lane == tp * NH + lax.broadcasted_iota(jnp.int32, (8, 32), 0)
    rates = jnp.sum(jnp.where(chosen, rate[...], 0.0), axis=1, keepdims=True)
    small = jnp.where(which < NH, -rates * soft, 1.0 / (1.0 + jnp.exp(-small)))
    row = lax.broadcasted_iota(jnp.int32, (8, 512), 0)
    lane = lax.broadcasted_iota(jnp.int32, (8, 512), 1) // 128
    logs = contract(small, (row == lane).astype(f32), ((0,), (0,)), HIGHEST)
    strengths = contract(small, (row == lane + NH).astype(f32), ((0,), (0,)), HIGHEST)
    for h in range(NH):
        gnew[h] = logs[0:32, head(h)]
        bnew[h] = strengths[0:32, head(h)]

    def rows_of(ref, t, h):
        return ref[h, pl.ds(t, 8, stride=4)]

    def unit_rows(m, factor):
        for h in range(NH):
            v = silu(summed(m, h))
            tmp[h] = v * lax.rsqrt(across(v * v) + epsilon) * factor
            for t in range(NT):
                kq[h, pl.ds(m * 4 + t, 8, stride=8)] = rows_of(tmp, t, h)

    second_sum(5)
    second_sum(6)
    last_sum(0)
    last_sum(1)
    unit_rows(0, 1.0)
    second_sum(7)
    last_sum(2)
    last_sum(3)
    unit_rows(1, 128**-0.5)

    @pl.loop(0, NB)
    def _(b):
        rows = pl.ds(pl.multiple_of(b * 8, 8), 8)
        for h in range(NH):
            left = kq[h, rows]
            large = left.astype(bf16).astype(f32)
            left = jnp.concatenate(
                [jnp.concatenate([large, large], axis=1), jnp.concatenate([left - large, jnp.zeros_like(left)], axis=1)],
                axis=0,
            )
            both = contract(left.astype(bf16), halves[b * NH + h], ((1,), (0,)))
            pbuf[h, rows] = both[0:8] + both[8:16]

    last_sum(4)
    last_sum(5)
    for h in range(NH):
        vnew[h] = silu(summed(2, h))
    for h in range(NH):
        keys = [every(kq, t, h) for t in range(NT)]
        written, decay = delta_rule(
            keys,
            [every(pbuf, t, h) for t in range(NT)],
            [rows_of(vnew, t, h) for t in range(NT)],
            [rows_of(gnew, t, h) for t in range(NT)],
            [rows_of(bnew, t, h) for t in range(NT)],
        )
        for t in range(NT):
            query = every(kq, 4 + t, h)
            attended = decay[t, -1] * every(pbuf, 4 + t, h) + across(keys[t] * query) * written[t]
            for i in range(t):
                attended = attended + decay[t, i] * across(keys[i] * query) * written[i]
            scaled = attended * lax.rsqrt(across(attended * attended) * (1.0 / 128) + epsilon)
            hout[h, pl.ds(t, 8, stride=4)] = scaled * hgain[...]

    for g in range(2):
        last_sum(6 + g)
        for h in (2 * g, 2 * g + 1):
            hsend[g, :, head(h - 2 * g)] = (hout[h] * silu(summed(3, h))).astype(bf16)
        for d in (4, 3, 5, 2, 6, 1, 7):
            go(remote(hsend.at[g], hz.at[g, d], hs.at[g], hr.at[g], at_z(z + d)))
        hz[g, 0] = hsend[g]

    arrive("wout", wobuf.at[:, 128:512], r_wo)
    arrive("heads0", hz.at[0, 1:8], hr.at[0])
    terms = jnp.dot(hz[0].reshape(256, 256), wobuf[0:256], preferred_element_type=f32)
    arrive("heads1", hz.at[1, 1:8], hr.at[1])
    terms = terms + jnp.dot(hz[1].reshape(256, 256), wobuf[256:512], preferred_element_type=f32)
    for d in range(NZ):
        zz = lax.rem(z + NZ - d, NZ)
        p3[lax.rem(zz, 2) * NY + zz // 2] = terms[d * 32 : (d + 1) * 32]
    go(remote(p3.at[pl.ds((1 - c) * NY, NY)], d2d, s_d2d, r_d2d, twin))
    arrive("twin", d2d, r_d2d)
    for j in range(NY):
        rows = p3[c * NY + j] + d2d[j]
        for e in range(NX):
            psend[j * NX + e] = rows[:, head(e)].astype(bf16)
    for ey, ex in (
        (2, 2), (2, 1), (2, 3), (1, 2), (3, 2), (2, 0), (0, 2), (1, 1), (1, 3), (3, 1), (3, 3), (1, 0), (3, 0), (0, 1), (0, 3),
    ):
        there = {"kv": z * NX + lax.rem(x + NX - ex, NX), "tp": lax.rem(y + ey, NY) * 2 + c}
        go(remote(psend.at[lax.rem(y + ey, NY) * NX + ex], precv.at[ey * NX + ex], s_part, r_part, there))
    own_part = p3[c * NY + y, :, 0:128] + d2d[y, :, 0:128]
    arrive("parts", precv.at[1:16], r_part)
    for ex in range(NX):
        total = own_part if ex == 0 else precv[ex].astype(f32)
        for ey in range(1, NY):
            total = total + precv[ey * NX + ex].astype(f32)
        mixed[lax.rem(x + ex, NX)] = total.astype(bf16)
    for ref, sem in (
        (xtok.at[1:4, mine], s_tok), (wbuf.at[0:2], s_direct), (wbuf.at[0], s_relay), (sqrecv, s_sq), (strecv, s_stat), (abrecv, s_small),
        (y1send, s_y1), (y2send, s_y2), (wobuf.at[:, 128:512], s_wo), (xtok.at[1:4, mine], s_twin), (d2d, s_d2d),
        (hz.at[0, 1:8], hs.at[0]), (hz.at[1, 1:8], hs.at[1]), (precv.at[1:16], s_part),
    ):
        arrive("drain", ref, sem)


def fused(*operands):
    anywhere = pl.BlockSpec(memory_space=pl.ANY)
    vmem = pl.BlockSpec(memory_space=pltpu.VMEM)
    dma = pltpu.SemaphoreType.DMA
    scratch = [
        pltpu.VMEM((NX * NZ, 128), f32),
        pltpu.VMEM((32, 512), bf16),
        pltpu.VMEM((32, 512), bf16),
        pltpu.VMEM((128, 128), bf16),
        pltpu.VMEM((128, 128), bf16),
        pltpu.VMEM((16, 8), f32),
        pltpu.VMEM((16, 8), f32),
        pltpu.VMEM((1, 8), jnp.int32),
        pltpu.VMEM((1, 32), f32),
        pltpu.VMEM((1, 128), f32),
        dma((10,)),
        pltpu.VMEM((128, 128), f32),
        pltpu.VMEM((128, 128), f32),
        pltpu.VMEM((NH, 64, 128), f32),
        pltpu.VMEM((8, 2048), f32),
        pltpu.VMEM((8, 2048), f32),
        pltpu.VMEM((16, 512), bf16),
        pltpu.VMEM((NX, 1, 128), f32),
        pltpu.VMEM((NZ, NX, 32, 128), bf16),
        pltpu.VMEM((NX, NZ, 32, 128), bf16),
        pltpu.VMEM((NX, 128, 2048), bf16),
        pltpu.VMEM((NX, 1, 256), f32),
        pltpu.VMEM((NX - 1, 1, 256), f32),
        pltpu.VMEM((1, 256), f32),
        pltpu.VMEM((NZ - 1, 1, 256), f32),
        pltpu.VMEM((NZ, 32, 128), f32),
        pltpu.VMEM((256, 512), bf16),
        pltpu.VMEM((NZ, 8, 128), f32),
        pltpu.VMEM((NZ - 1, 8, 128), f32),
        pltpu.VMEM((128, 2048), f32),
        pltpu.VMEM((128, 2048), bf16),
        pltpu.VMEM((128, 2048), bf16),
        pltpu.VMEM((3, 32, 2048), bf16),
        pltpu.VMEM((3, 32, 2048), bf16),
        pltpu.VMEM((512, 512), bf16),
        pltpu.VMEM((NB * NH, 256, 128), bf16),
        pltpu.VMEM((NH, 64, 128), f32),
        pltpu.VMEM((NH, 64, 128), f32),
        pltpu.VMEM((NH, 64, 128), f32),
        pltpu.VMEM((NH, 32, 128), f32),
        pltpu.VMEM((NH, 64, 128), f32),
        pltpu.VMEM((NH, 32, 128), f32),
        pltpu.VMEM((NH, 32, 128), f32),
        pltpu.VMEM((NH, 32, 128), f32),
        pltpu.VMEM((NH, 32, 128), f32),
        pltpu.VMEM((2, 32, 256), bf16),
        pltpu.VMEM((2, NZ, 32, 256), bf16),
        pltpu.VMEM((NZ, 32, 512), f32),
        pltpu.VMEM((NY, 32, 512), f32),
        pltpu.VMEM((NY * NX, 32, 128), bf16),
        pltpu.VMEM((NY * NX, 32, 128), bf16),
        dma((3 + NC,)),
        dma((3,)),
        dma((NC, 2)),
        dma((NC,)),
        dma((NC,)),
        dma((NC,)),
        dma((2,)),
        dma((2,)),
        dma((12,)),
        dma((7,)),
        pltpu.SemaphoreType.REGULAR((3,)),
    ]
    return pl.pallas_call(
        kernel,
        out_shape=(
            pltpu.VMEM((NX, 32, 128), bf16),
            pltpu.VMEM((NB * NH, 128, 128), f32),
        ),
        in_specs=[anywhere] * 17,
        out_specs=(vmem, vmem),
        scratch_shapes=scratch,
        compiler_params=pltpu.CompilerParams(collective_id=0, has_side_effects=True),
        name="step",
    )(*operands)


def per_device(
    tokens,
    norm_gain,
    w_query,
    w_key,
    w_value,
    w_gate,
    w_decay,
    w_beta,
    decay_rate,
    head_gain,
    w_out,
    state,
    prev_keys,
    prev_values,
    prev_log_decay,
    prev_beta,
    accepted,
):
    mixed, carried = fused(
        tokens.reshape(NZ, NX, 32, 128), w_key, w_query, w_value, w_gate, w_out,
        state.reshape(NB * NH, 128, 128), norm_gain.reshape(NX * NZ, 128), w_decay.T, w_beta.T,
        prev_keys.reshape(128, 128), prev_values.reshape(128, 128),
        prev_log_decay.transpose(1, 2, 0).reshape(16, NB), prev_beta.transpose(1, 2, 0).reshape(16, NB),
        accepted.reshape(1, NB), decay_rate.reshape(1, 32), head_gain.reshape(1, 128),
    )
    return mixed.reshape(32, NT, 128), carried.reshape(NB, NH, 128, 128)


def solution(mesh):
    placed = (
        P(None, None, "kv"),
        P(),
        P("kv", "tp"),
        P("kv", "tp"),
        P("kv", "tp"),
        P("kv", "tp"),
        P(),
        P(),
        P(),
        P(),
        P("tp", "kv"),
        P("kv", "tp", None, None),
        P("kv", "tp", None, None),
        P("kv", "tp", None, None),
        P("kv", "tp", None),
        P("kv", "tp", None),
        P("kv"),
    )
    return jax.shard_map(
        per_device,
        mesh=mesh,
        in_specs=placed,
        out_specs=(P("tp", None, "kv"), P("kv", "tp", None, None)),
        check_vma=False,
    )
```

time: 64.1 us -> 57.7 us (0.900)
  Pallas kernels: 61.3 us -> 55 us
    pallas_call x1, Pallas kernels: 61.3 us -> 55 us  [fused(): pl.pallas_call(kernel, out_shape=(pltpu.VMEM((NX, 32, 128), bf16), pltpu....]
where the time goes in v4:
time: 57.7 us; the launch traced here: 57.6 us
  Pallas kernels  55 us (95%)
  local copies, waits for them, and re-layouts  1.94 us (3%)
  between operations  0.65 us (1%)
    pallas_call x1, Pallas kernels, fused(): pl.pallas_call(kernel, out_shape=(pltpu.VMEM((NX, 32, 128), bf16), pltpu....  55 us
    unnamed x2, local copies, waits for them, and re-layouts  1.94 us

profile of v4, /device:TPU:1, one launch (start us, length us, event | category | flops | bytes accessed | tf_op | source)
XLA Modules:
  0.0 57.6 jit_solution(4373518813433886240)
XLA Ops:
  0.6 55.0 %step.1 = (bf16[4,32,128]{2,1,0:T(8,128)(2,1)S(1)}, f32[32,128,128]{2,1,0:T(8,128)S(1)}) custom-call(bf16[8,4,32,128]{3,2,1,0:T(8,128)(2,1)} %bitcast.21, bf16[128,512]{1,0:T(8,128)(2,1)} %wkey.1, bf16[128,512]{1,0:T(8,128)(2,1)} %wquery.1, bf16[128,512]{1,0:T(8,128)(2,1)} %wvalue.1, bf16[128,512]{1,0:T(8,128)(2,1)} %wgate.1, bf16[512,128]{1,0:T(8,128)(2,1)} %wout.1, ...), custom_call_target="tpu_custom_call" | custom-call | tf_op jit(solution)/shard_map/step/pallas_call | solution.py:522
  55.7 0.6 %copy.21 = bf16[32,4,128]{2,1,0:T(4,128)(2,1)} copy(bf16[32,4,128]{2,1,0:T(4,128)(2,1)S(1)} %bitcast.19) | data formatting | bytes 65536
  56.3 1.3 %copy.22 = f32[8,4,128,128]{3,2,1,0:T(8,128)} copy(f32[8,4,128,128]{3,2,1,0:T(8,128)S(1)} %bitcast.18) | data formatting | bytes 4194304

commit v5 on v4

--- a/solution.py
+++ b/solution.py
@@ -334,8 +334,8 @@
     project(6)
     second_sum(3)
     project(7)
+    second_sum(4)
     update_state(5, NB)
-    second_sum(4)
 
     arrive("small", abrecv, r_small)
     small = absend[0]
@@ -533,6 +533,31 @@
     )(*operands)
 
 
+def to_hbm(mixed, carried):
+    parts = 4
+
+    def body(mixed, carried, mixed_out, carried_out, sems):
+        size = carried.shape[0] // parts
+        copies = [pltpu.make_async_copy(mixed, mixed_out, sems.at[parts])]
+        for i in range(parts):
+            rows = pl.ds(i * size, size)
+            copies.append(pltpu.make_async_copy(carried.at[rows], carried_out.at[rows], sems.at[i]))
+        for copy in copies:
+            copy.start()
+        for copy in copies:
+            copy.wait()
+
+    vmem, hbm = pl.BlockSpec(memory_space=pltpu.VMEM), pl.BlockSpec(memory_space=pltpu.HBM)
+    return pl.pallas_call(
+        body,
+        out_shape=tuple(pltpu.HBM(a.shape, a.dtype) for a in (mixed, carried)),
+        in_specs=[vmem, vmem],
+        out_specs=(hbm, hbm),
+        scratch_shapes=[pltpu.SemaphoreType.DMA((parts + 1,))],
+        name="to_hbm",
+    )(pltpu.with_memory_space_constraint(mixed, pltpu.VMEM), pltpu.with_memory_space_constraint(carried, pltpu.VMEM))
+
+
 def per_device(
     tokens,
     norm_gain,
@@ -559,6 +584,7 @@
         prev_log_decay.transpose(1, 2, 0).reshape(16, NB), prev_beta.transpose(1, 2, 0).reshape(16, NB),
         accepted.reshape(1, NB), decay_rate.reshape(1, 32), head_gain.reshape(1, 128),
     )
+    mixed, carried = to_hbm(mixed, carried)
     return mixed.reshape(32, NT, 128), carried.reshape(NB, NH, 128, 128)
 
 

time: 57.7 us -> 56.3 us (0.976)
  local copies, waits for them, and re-layouts: 1.94 us -> 0 us
    unnamed x2 -> x0, local copies, waits for them, and re-layouts: 1.94 us -> none
    pallas_call x0 -> x1, Pallas kernels: none -> 1.37 us  [to_hbm(): pl.pallas_call(body, out_shape=tuple((pltpu.HBM(a.shape, a.dtype) for a i...]
    pallas_call x1, Pallas kernels: 55 us -> 54.2 us  [fused(): pl.pallas_call(kernel, out_shape=(pltpu.VMEM((NX, 32, 128), bf16), pltpu....]
where the time goes in v5:
time: 56.3 us; the launch traced here: 56.2 us
  Pallas kernels  55.5 us (99%)
  between operations  0.65 us (1%)
    pallas_call x1, Pallas kernels, fused(): pl.pallas_call(kernel, out_shape=(pltpu.VMEM((NX, 32, 128), bf16), pltpu....  54.2 us
    pallas_call x1, Pallas kernels, to_hbm(): pl.pallas_call(body, out_shape=tuple((pltpu.HBM(a.shape, a.dtype) for a i...  1.37 us

profile of v5, /device:TPU:1, one launch (start us, length us, event | category | flops | bytes accessed | tf_op | source)
XLA Modules:
  0.0 56.2 jit_solution(2054869268839700206)
XLA Ops:
  0.6 54.2 %step.1 = (bf16[4,32,128]{2,1,0:T(8,128)(2,1)S(1)}, f32[32,128,128]{2,1,0:T(8,128)S(1)}) custom-call(bf16[8,4,32,128]{3,2,1,0:T(8,128)(2,1)} %bitcast.19, bf16[128,512]{1,0:T(8,128)(2,1)} %wkey.1, bf16[128,512]{1,0:T(8,128)(2,1)} %wquery.1, bf16[128,512]{1,0:T(8,128)(2,1)} %wvalue.1, bf16[128,512]{1,0:T(8,128)(2,1)} %wgate.1, bf16[512,128]{1,0:T(8,128)(2,1)} %wout.1, ...), custom_call_target="tpu_custom_call" | custom-call | tf_op jit(solution)/shard_map/step/pallas_call | solution.py:522
  54.8 1.4 %to_hbm.1 = (bf16[4,32,128]{2,1,0:T(8,128)(2,1)}, f32[32,128,128]{2,1,0:T(8,128)}) custom-call(bf16[4,32,128]{2,1,0:T(8,128)(2,1)S(1)} %get-tuple-element.6.mixed, f32[32,128,128]{2,1,0:T(8,128)S(1)} %get-tuple-element.7.carried), custom_call_target="tpu_custom_call" | custom-call | tf_op jit(solution)/shard_map/to_hbm/pallas_call | solution.py:551

commit v6 on v5

--- a/solution.py
+++ b/solution.py
@@ -317,11 +317,10 @@
     direct(7)
     project(2)
     relay(5)
-    update_state(2, 3)
     project(3)
     second_sum(0)
     relay(6)
-    update_state(3, 4)
+    update_state(2, 4)
     second_sum(1)
     project(4)
     relay(7)

time: 56.3 us -> 55.9 us (level)
  no operation moved by 1% of the time
where the time goes in v6:
time: 55.9 us
  Pallas kernels  55.2 us (99%)
  between operations  0.65 us (1%)
    pallas_call x1, Pallas kernels, fused(): pl.pallas_call(kernel, out_shape=(pltpu.VMEM((NX, 32, 128), bf16), pltpu....  53.8 us
    pallas_call x1, Pallas kernels, to_hbm(): pl.pallas_call(body, out_shape=tuple((pltpu.HBM(a.shape, a.dtype) for a i...  1.37 us

profile of v6, /device:TPU:1, one launch (start us, length us, event | category | flops | bytes accessed | tf_op | source)
XLA Modules:
  0.0 55.9 jit_solution(4666459593708761333)
XLA Ops:
  0.6 53.8 %step.1 = (bf16[4,32,128]{2,1,0:T(8,128)(2,1)S(1)}, f32[32,128,128]{2,1,0:T(8,128)S(1)}) custom-call(bf16[8,4,32,128]{3,2,1,0:T(8,128)(2,1)} %bitcast.19, bf16[128,512]{1,0:T(8,128)(2,1)} %wkey.1, bf16[128,512]{1,0:T(8,128)(2,1)} %wquery.1, bf16[128,512]{1,0:T(8,128)(2,1)} %wvalue.1, bf16[128,512]{1,0:T(8,128)(2,1)} %wgate.1, bf16[512,128]{1,0:T(8,128)(2,1)} %wout.1, ...), custom_call_target="tpu_custom_call" | custom-call | tf_op jit(solution)/shard_map/step/pallas_call | solution.py:521
  54.5 1.4 %to_hbm.1 = (bf16[4,32,128]{2,1,0:T(8,128)(2,1)}, f32[32,128,128]{2,1,0:T(8,128)}) custom-call(bf16[4,32,128]{2,1,0:T(8,128)(2,1)S(1)} %get-tuple-element.6.mixed, f32[32,128,128]{2,1,0:T(8,128)S(1)} %get-tuple-element.7.carried), custom_call_target="tpu_custom_call" | custom-call | tf_op jit(solution)/shard_map/to_hbm/pallas_call | solution.py:550
